TPU v7x, 512 devices: a whole 4x8x8 slice. The times are simulated.
512 devices in a mesh: sp: 32 (over z, x), tp: 16 (over y, core).
Axes of the slice: x: 4, y: 8, z: 8, core: 2. Of those that a mesh axis runs over, the one named last changes fastest.
Arguments:
- probe_vectors: bfloat16 [4096, 2048], P('sp', 'tp'), may hold values from -6 to 6
- address_vectors: bfloat16 [4096, 2048], P('sp', 'tp'), may hold values from -6 to 6
- content_vectors: bfloat16 [4096, 2048], P('sp', 'tp'), may hold values from -6 to 6
- storage_raw_signal: float32 [16, 4096], P('tp', 'sp'), may hold values from -8 to 4
- fade_raw_signal: float32 [16, 4096], P('tp', 'sp'), may hold values from -6 to 6
- channel_fade_exponent: float32 [16], P('tp'), may hold values from -9 to 0
- extra_fade_amount: float32 [16, 4096], P('tp', 'sp'), may hold values from -1 to 0
- sequence_label: int32 [4096], P('sp'), may hold values from 0 to 8, never falling along the last dimension, each value on 1 to 768 neighbouring positions
- exit_valve_raw_signal: bfloat16 [4096, 2048], P('sp', 'tp'), may hold values from -6 to 6
- final_projection_matrix: bfloat16 [2048, 2048], P('tp'), may hold values from -0.125 to 0.125
- incoming_rows_matrix: bfloat16 [4096, 2048], P('sp', 'tp'), may hold values from -48 to 48
- initial_rescale_factor: float32 [2048], P('tp'), may hold values from 0 to 3
- specialist_picks: int32 [4096, 2], P('sp'), may hold values from 0 to 31, all different within a row; in each aligned block of 128 rows (0 to 127, 128 to 255, ...) at most 9 rows name the same one
- picked_specialist_share: bfloat16 [4096, 2], P('sp'), may hold values from 0.29882812 to 1.1953125
- specialist_valve_matrix: bfloat16 [32, 2048, 4096], P('sp', None, 'tp'), may hold values from -0.125 to 0.125
- specialist_raising_matrix: bfloat16 [32, 2048, 4096], P('sp', None, 'tp'), may hold values from -0.125 to 0.125
- specialist_lowering_matrix: bfloat16 [32, 4096, 2048], P('sp', 'tp'), may hold values from -0.09375 to 0.09375
- common_valve_matrix: bfloat16 [2048, 512], P(None, 'tp'), may hold values from -0.125 to 0.125
- common_raising_matrix: bfloat16 [2048, 512], P(None, 'tp'), may hold values from -0.125 to 0.125
- common_lowering_matrix: bfloat16 [512, 2048], P('tp'), may hold values from -0.25 to 0.25
- latter_rescale_factor: float32 [2048], P('tp'), may hold values from 0.1 to 1.9
Outputs:
- result: bfloat16 [4096, 2048], P('sp', 'tp')
Inputs may be any that keep to these rules, and one draw needn't show every extreme that they name: `sequence_label`: document numbers never fall; a document has 1 to 768 positions, one exactly 768. `specialist_picks`: each row names 2 different experts; among the rows of one index of sp no expert is named more than 9 times, a bound that some block reaches.
All inputs are finite; a program needn't handle non-finite values.
Results may differ from a plain program's by a relative error of at most 0.018.
Values may be sent and summed in bfloat16 or wider, within the bound.
A program may use at most 64 MiB of HBM per device.

v0:
```python
import jax
import jax.numpy as jnp
from jax import lax
from jax.sharding import Mesh
from jax.sharding import PartitionSpec as P

DK = 128
DV = 128
BLOCK = 64
SP = ("sp_0", "sp_1")


ALPHA = 2.0**0.25


def sent_to_all(value, axis):
    peers = lax.axis_size(axis)
    return lax.all_to_all(
        jnp.broadcast_to(value[None], (peers, *value.shape)), axis, 0, 0, tiled=True
    )


def over_copies(value, axis):
    return sent_to_all(value, axis).sum(axis=0)


def together(arrays, axis):
    flat, at, outs = (jnp.concatenate([a.reshape(-1) for a in arrays]), 0, [])
    subtotal = over_copies(flat, axis)
    for a in arrays:
        outs.append(subtotal[at : at + a.size].reshape(a.shape))
        at += a.size
    return tuple(outs)


def nothing_yet(value, identity):
    return jax.tree.map(
        lambda part, zero: jnp.zeros_like(part) + jnp.asarray(zero, part.dtype), value, identity
    )


def collected_together(value, axis):
    leaves = jax.tree.leaves(value)
    turns = sorted(range(len(leaves)), key=lambda k: -leaves[k].size)
    width = (1, *leaves[turns[0]].shape)[-1]
    lines = [
        jnp.pad(leaves[k].reshape(-1), (0, -leaves[k].size % width)).reshape(-1, width)
        for k in turns
    ]
    both, at, found = (lax.all_gather(jnp.concatenate(lines), axis), 0, {})
    for k, line in zip(turns, lines):
        piece = both[:, at : at + len(line)].reshape(len(both), -1)
        found[k] = piece[:, : leaves[k].size].reshape(-1, *leaves[k].shape)
        at += len(line)
    numbers = iter(range(len(leaves)))
    return jax.tree.map(lambda _: found[next(numbers)], value)


def prefix_by_axis(value, axes, combine, identity):
    before = start = nothing_yet(value, identity)
    subtotal = value
    for axis in reversed(axes):
        peers, mine = (lax.axis_size(axis), lax.axis_index(axis))
        pieces = collected_together(
            jax.tree.map(
                lambda part, kind: part.astype(kind),
                subtotal,
                (jnp.bfloat16, jnp.bfloat16, jnp.bfloat16, jnp.bfloat16),
            ),
            axis,
        )
        inside, subtotal = (start, start)
        for k in range(peers):
            passed = k < mine
            subtotal = combine(
                subtotal, jax.tree.map(lambda part, own: part[k].astype(own.dtype), pieces, value)
            )
            inside = jax.tree.map(lambda new, old: jnp.where(passed, new, old), subtotal, inside)
        before = combine(inside, before)
    return before


def cut_along(value, dim, peers):
    before, after = (value.shape[:dim], value.shape[dim + 1 :])
    return jnp.moveaxis(value.reshape(*before, peers, -1, *after), dim, 0)


def sent_and_summed(value, axis, dim):
    pieces = cut_along(value, dim, lax.axis_size(axis))
    arrived = lax.all_to_all(pieces, axis, split_axis=0, concat_axis=0, tiled=True)
    return arrived.astype(jnp.float32).sum(axis=0)


def in_order(pieces, dim):
    pieces = jnp.moveaxis(pieces, 0, dim)
    lengths = pieces.shape
    return pieces.reshape(*lengths[:dim], lengths[dim] * lengths[dim + 1], *lengths[dim + 2 :])


def collect(value, axis, dim):
    return in_order(sent_to_all(value, axis), dim)


def unit_rows(array):
    return array * lax.rsqrt(jnp.sum(array * array, -1, keepdims=True) + 1e-06)


def matmul_high(form, left, right):
    return jnp.einsum(form, left, right)


def feature_norm(summed, gain):
    width = summed.shape[-1] * lax.axis_size("tp")
    totals, squares = together((jnp.sum(summed, -1), jnp.sum(summed * summed, -1)), "tp")
    row_mean = totals / width
    row_var = squares / width - row_mean * row_mean
    return (summed - row_mean[:, None]) * lax.rsqrt(row_var[:, None] + 1e-05) * gain


def compose(earlier, later):
    first_map, first_shift, first_doc, first_last = earlier
    second_map, second_shift, second_doc, second_last = later
    joined = ((second_doc == first_last) | (first_last < 0) | (second_doc < 0)).astype(jnp.float32)
    new_map = joined * matmul_high("hij,hjk->hik", second_map, first_map)
    new_shift = joined * matmul_high("hij,hjk->hik", second_map, first_shift) + second_shift
    new_doc = jnp.where(first_doc < 0, second_doc, first_doc)
    new_last = jnp.where(second_last < 0, first_last, second_last)
    return (new_map, new_shift, new_doc, new_last)


def block_pass(query_unit, key_unit, write_gate, decay_logarithm, segment, values_in, initial):
    heads_here, blocks, block_len, key_depth = query_unit.shape
    cumulative = jnp.cumsum(decay_logarithm, -1)
    before = jnp.concatenate([segment[:1, 0], segment[:-1, -1]])
    carried = (segment == before[:, None]).astype(jnp.float32)
    same_doc = segment[:, :, None] == segment[:, None, :]
    offsets = jnp.arange(block_len)
    lower_tri = offsets[:, None] >= offsets[None, :]
    strict = offsets[:, None] > offsets[None, :]
    log_gap = cumulative[..., :, None] - cumulative[..., None, :]
    reach_mask = jnp.where(lower_tri & same_doc, jnp.exp(jnp.where(lower_tri, log_gap, 0.0)), 0.0)
    weighted_keys = key_unit * write_gate[..., None]
    coupling = jnp.where(
        strict, matmul_high("hncd,hnsd->hncs", weighted_keys, key_unit) * reach_mask, 0.0
    )
    identity_block = jnp.eye(block_len, dtype=jnp.float32)
    inverse = identity_block - coupling
    nil_power = coupling
    for squaring in range(block_len.bit_length() - 2):
        nil_power = matmul_high("hncs,hnst->hnct", nil_power, nil_power)
        inverse = matmul_high("hncs,hnst->hnct", inverse, identity_block + nil_power)
    growth = jnp.exp(cumulative) * carried
    update = matmul_high("hncs,hnse->hnce", inverse, values_in * write_gate[..., None])
    correction = matmul_high("hncs,hnsd->hncd", inverse, weighted_keys * growth[..., None])
    final_growth = jnp.exp(cumulative[..., -1]) * (segment[:, -1] == before).astype(jnp.float32)
    tail_decay = jnp.exp(cumulative[..., -1:] - cumulative) * (segment == segment[:, -1:]).astype(
        jnp.float32
    )
    tail_keys = key_unit * tail_decay[..., None]
    query_grown = query_unit * growth[..., None]
    local_scores = matmul_high("hncd,hnsd->hncs", query_unit, key_unit) * reach_mask

    def advance(carry_state, inputs):
        grown_query, block_corr, block_update, block_keys, block_scores, block_fade = inputs
        fresh_values = block_update - matmul_high("hcd,hde->hce", block_corr, carry_state)
        next_state = carry_state * block_fade[:, None, None] + matmul_high(
            "hcd,hce->hde", block_keys, fresh_values
        )
        block_out = matmul_high("hcd,hde->hce", grown_query, carry_state) + matmul_high(
            "hcs,hse->hce", block_scores, fresh_values
        )
        return (next_state, block_out)

    inputs = tuple(
        (
            jnp.moveaxis(array, 1, 0)
            for array in (query_grown, correction, update, tail_keys, local_scores, final_growth)
        )
    )
    final_state, outputs = lax.scan(advance, initial, inputs)
    outputs = jnp.moveaxis(outputs, 0, 1).reshape(heads_here, blocks * block_len, -1)
    return (final_state, outputs)


def shards(
    probe_vectors,
    address_vectors,
    content_vectors,
    storage_raw_signal,
    fade_raw_signal,
    channel_fade_exponent,
    extra_fade_amount,
    sequence_label,
    exit_valve_raw_signal,
    final_projection_matrix,
    incoming_rows_matrix,
    initial_rescale_factor,
    specialist_picks,
    picked_specialist_share,
    specialist_valve_matrix,
    specialist_raising_matrix,
    specialist_lowering_matrix,
    common_valve_matrix,
    common_raising_matrix,
    common_lowering_matrix,
    latter_rescale_factor,
):
    tokens_here = probe_vectors.shape[0]
    heads_here = storage_raw_signal.shape[0]
    blocks = tokens_here // BLOCK

    def split_heads(array, width):
        moved = jnp.transpose(
            array.astype(jnp.float32).reshape(tokens_here, heads_here, width), (1, 0, 2)
        )
        return moved.reshape(heads_here, blocks, BLOCK, width)

    query_unit = unit_rows(split_heads(probe_vectors, DK)) * DK ** (-0.5)
    key_unit = unit_rows(split_heads(address_vectors, DK))
    value_rows = split_heads(content_vectors, DV)
    write_gate = jax.nn.sigmoid(storage_raw_signal).reshape(heads_here, blocks, BLOCK)
    decay_logarithm = (
        extra_fade_amount
        - jnp.exp(channel_fade_exponent)[:, None] * jax.nn.softplus(fade_raw_signal)
    ).reshape(heads_here, blocks, BLOCK)
    segment = sequence_label.astype(jnp.float32).reshape(blocks, BLOCK)
    extended = jnp.concatenate(
        [value_rows, jnp.zeros((heads_here, blocks, BLOCK, DK), jnp.float32)], -1
    )
    identity_state = jnp.broadcast_to(jnp.eye(DK, dtype=jnp.float32), (heads_here, DK, DK))
    start_state = jnp.concatenate(
        [jnp.zeros((heads_here, DK, DV), jnp.float32), identity_state], -1
    )
    summary, local_out = block_pass(
        query_unit, key_unit, write_gate, decay_logarithm, segment, extended, start_state
    )
    first_doc = segment[0, 0]
    last_doc = segment[-1, -1]
    empty_doc = jnp.full((), -1.0, jnp.float32)
    prefix = prefix_by_axis(
        (summary[..., DV:], summary[..., :DV], first_doc, last_doc),
        SP,
        compose,
        (identity_state, jnp.zeros((heads_here, DK, DV), jnp.float32), empty_doc, empty_doc),
    )
    incoming = prefix[1] * (first_doc == prefix[3]).astype(jnp.float32)
    memory_layer_result = local_out[..., :DV] + matmul_high(
        "hcd,hde->hce", local_out[..., DV:], incoming
    )
    scaled = memory_layer_result * lax.rsqrt(
        jnp.mean(memory_layer_result * memory_layer_result, -1, keepdims=True) + 1e-06
    )
    token_major = jnp.transpose(scaled, (1, 0, 2)).reshape(tokens_here, heads_here * DV)
    heads_out = (token_major * jax.nn.silu(exit_valve_raw_signal.astype(jnp.float32))).astype(
        jnp.bfloat16
    )
    partial_proj = jnp.dot(heads_out, final_projection_matrix, preferred_element_type=jnp.float32)
    projected = sent_and_summed(partial_proj.astype(jnp.bfloat16), "tp", 1)
    middle = feature_norm(
        ALPHA * incoming_rows_matrix.astype(jnp.float32) + projected, initial_rescale_factor
    ).astype(jnp.bfloat16)
    top = specialist_picks.shape[1]
    local_experts = specialist_valve_matrix.shape[0]
    experts_all = local_experts * lax.axis_size(SP)
    capacity = max(2, 9 * tokens_here * top // (8 * experts_all))
    picks = tokens_here * top
    flat_routes = specialist_picks.reshape(picks)
    one_hot = (flat_routes[:, None] == jnp.arange(experts_all, dtype=jnp.int32)[None, :]).astype(
        jnp.int32
    )
    rank_in = jnp.sum(jnp.cumsum(one_hot, 0) * one_hot, 1) - 1
    slot_of = flat_routes * capacity + rank_in
    owner = (
        jnp.full((experts_all * capacity,), picks, jnp.int32)
        .at[slot_of]
        .set(jnp.arange(picks, dtype=jnp.int32))
    )
    live = owner < picks
    safe_owner = jnp.minimum(owner, picks - 1)
    source_row = safe_owner // top
    slot_weight = jnp.where(
        live, picked_specialist_share.reshape(picks)[safe_owner], jnp.zeros((), jnp.bfloat16)
    )
    slot_shared = jnp.where(live & (safe_owner % top == 0), 1.0, 0.0).astype(jnp.bfloat16)
    slot_info = jnp.stack([slot_weight, slot_shared], -1).reshape(experts_all, capacity, 2)
    sent = jnp.where(live[:, None], middle[source_row], jnp.zeros((), jnp.bfloat16)).reshape(
        experts_all, capacity, -1
    )
    arrived = lax.all_to_all(sent, SP, split_axis=0, concat_axis=0, tiled=True)
    info = lax.all_to_all(slot_info, SP, split_axis=0, concat_axis=0, tiled=True)
    arrived = collect(arrived, "tp", 2)
    slot_count = arrived.shape[1]
    sources = arrived.shape[0] // local_experts
    grouped = arrived.reshape(sources, local_experts, slot_count, arrived.shape[2])
    info_grouped = info.astype(jnp.float32).reshape(sources, local_experts, slot_count, 2)
    inputs_e = grouped[:, 0].reshape(sources * slot_count, -1)
    weight_e = info_grouped[:, 0, :, 0].reshape(-1, 1)
    shared_e = info_grouped[:, 0, :, 1].reshape(-1, 1)
    gate_e = jnp.dot(inputs_e, specialist_valve_matrix[0], preferred_element_type=jnp.float32)
    up_e = jnp.dot(inputs_e, specialist_raising_matrix[0], preferred_element_type=jnp.float32)
    hidden_e = (jax.nn.silu(gate_e) * up_e * weight_e).astype(jnp.bfloat16)
    shared_g = jnp.dot(inputs_e, common_valve_matrix, preferred_element_type=jnp.float32)
    shared_u = jnp.dot(inputs_e, common_raising_matrix, preferred_element_type=jnp.float32)
    shared_hidden = (jax.nn.silu(shared_g) * shared_u * shared_e).astype(jnp.bfloat16)
    partial_out = jnp.dot(
        hidden_e, specialist_lowering_matrix[0], preferred_element_type=jnp.float32
    )
    partial_out = partial_out + jnp.dot(
        shared_hidden, common_lowering_matrix, preferred_element_type=jnp.float32
    )
    results = partial_out.reshape(sources, 1, slot_count, -1)
    partials = results.reshape(sources, slot_count, -1)
    summed = sent_and_summed(partials.astype(jnp.bfloat16), "tp", 2).astype(jnp.bfloat16)
    returned = lax.all_to_all(summed, SP, split_axis=0, concat_axis=0, tiled=True)
    per_route = (
        returned.reshape(experts_all * capacity, -1)[slot_of]
        .astype(jnp.float32)
        .reshape(tokens_here, top, -1)
    )
    mixture = jnp.sum(per_route, 1)
    second_sum = ALPHA * middle.astype(jnp.float32) + mixture
    return feature_norm(second_sum, latter_rescale_factor).astype(jnp.bfloat16)


def solution(mesh):
    torus = Mesh(mesh.devices.reshape(8, 4, mesh.shape["tp"]), ("sp_0", "sp_1", "tp"))
    return jax.shard_map(
        shards,
        mesh=torus,
        in_specs=(
            P(SP, "tp"),
            P(SP, "tp"),
            P(SP, "tp"),
            P("tp", SP),
            P("tp", SP),
            P("tp"),
            P("tp", SP),
            P(SP),
            P(SP, "tp"),
            P("tp", None),
            P(SP, "tp"),
            P("tp"),
            P(SP, None),
            P(SP, None),
            P(SP, None, "tp"),
            P(SP, None, "tp"),
            P(SP, "tp", None),
            P(None, "tp"),
            P(None, "tp"),
            P("tp", None),
            P("tp"),
        ),
        out_specs=P(SP, "tp"),
        check_vma=False,
    )
```

profile of v0, /device:TPU:1, one launch (start us, length us, event | category | flops | bytes accessed | tf_op | source)
XLA Modules:
  0.0 279.6 jit_solution(17062271697256042862)
XLA Ops:
  0.0 0.9 convert_element_type.399
  0.9 0.9 multiply_reduce_fusion.4
  1.8 0.8 convert_element_type.401
  2.5 0.9 multiply_reduce_fusion.3
  4.1 0.7 divide_reduce_fusion
  4.9 0.7 convert_element_type.398
  5.9 0.6 fusion.211
  8.3 1.5 slice_reduce_fusion.4
  9.8 1.4 pad_maximum_fusion.3
  12.4 3.4 %while.12 = (s32[]{:T(128)}, f32[1,128,256]{2,1,0:T(8,128)S(1)}, f32[2,1,64,256]{3,2,1,0:T(8,128)S(1)}, f32[2,1]{1,0:T(2,128)S(1)}, bf16[2,1,64,128]{3,2,1,0:T(8...) while((s32[]{:T(128)}, f32[1,128,256]{2,1,0:T(8,128)S(1)}, ...), condition=%wide.region_4.5_spmd, body=%wide.region_3.4_spmd.sunk | while | flops 14794754 | bytes 952445 | solution.py:180
  13.3 0.8 fusion.279
  15.0 0.8 fusion.279
  16.4 0.6 pad_bitcast_fusion.2
  17.8 10.6 %all-gather.2 = bf16[4,258,128]{2,1,0:T(8,128)(2,1)S(1)} all-gather(bf16[1,258,128]{2,1,0:T(8,128)(2,1)S(1)} %maximum_bitcast_fusion), channel_id=2, replica_groups=mesh['sp_0'=8,'sp_1'=4,'tp'=16] {'sp_1'}, dimensions={0}, use_global_device_ids=true | all-gather | bytes 330240 | tf_op jit(solution)/shard_map/all_gather | solution.py:50
  28.4 0.6 fusion.210
  29.6 0.6 fusion.209
  43.3 26.6 %all-gather.3 = bf16[8,258,128]{2,1,0:T(8,128)(2,1)S(1)} all-gather(bf16[1,258,128]{2,1,0:T(8,128)(2,1)S(1)} %maximum_bitcast_fusion.1), channel_id=3, replica_groups=mesh['sp_0'=8,'sp_1'=4,'tp'=16] {'sp_0'}, dimensions={0}, use_global_device_ids=true | all-gather | bytes 594432 | tf_op jit(solution)/shard_map/all_gather | solution.py:50
  69.9 0.6 fusion.207
  80.7 0.6 fusion.208
  93.1 0.9 copy.210
  94.0 16.1 %all-to-all-start = ((bf16[16,128,128]{2,1,0:T(8,128)(2,1)}), bf16[16,128,128]{2,1,0:T(8,128)(2,1)S(1)}, u32[]{:S(2)}, u32[]{:S(2)}) async-start(bf16[16,128,128]{2,1,0:T(8,128)(2,1)} %bitcast.376), calls=%async_computation | async-start | bytes 1048576 | tf_op jit(solution)/shard_map/all_to_all | solution.py:90
  110.6 0.6 reduce-window.6
  112.1 1.4 scatter_custom_fusion
  113.5 2.4 gather_fusion.1
  115.9 11.4 %all-to-all-done = bf16[16,128,128]{2,1,0:T(8,128)(2,1)S(1)} async-done(((bf16[16,128,128]{2,1,0:T(8,128)(2,1)}), bf16[16,128,128]{2,1,0:T(8,128)(2,1)S(1)}, u32[]{:S(2)}, u32[]{:S(2)}) %all-to-all-start) | async-done | bytes 524320 | tf_op jit(solution)/shard_map/all_to_all | solution.py:90
  127.6 0.6 broadcast_in_dim.56
  128.2 3.4 %all-to-all-start.1 = ((f32[16,1,256]{2,1,0:T(1,128)}), f32[16,1,256]{2,1,0:T(1,128)S(1)}, u32[]{:S(2)}, u32[]{:S(2)}) async-start(f32[16,1,256]{2,1,0:T(1,128)} %broadcast_in_dim.56), calls=%async_computation.1 | async-start | bytes 32768 | tf_op jit(solution)/shard_map/all_to_all | solution.py:18
  131.7 6.8 %all-to-all-done.1 = f32[16,1,256]{2,1,0:T(1,128)S(1)} async-done(((f32[16,1,256]{2,1,0:T(1,128)}), f32[16,1,256]{2,1,0:T(1,128)S(1)}, u32[]{:S(2)}, u32[]{:S(2)}) %all-to-all-start.1) | async-done | bytes 16416 | tf_op jit(solution)/shard_map/all_to_all | solution.py:18
  138.7 1.4 gather_fusion
  140.1 0.8 broadcast_select_fusion
  140.9 5.9 %all-to-all-start.2 = ((bf16[32,9,128]{2,1,0:T(8,128)(2,1)}), bf16[32,9,128]{2,1,0:T(8,128)(2,1)S(1)}, u32[]{:S(2)}, u32[]{:S(2)}) async-start(bf16[32,9,128]{2,1,0:T(8,128)(2,1)} %broadcast_select_fusion), calls=%async_computation.2 | async-start | bytes 262144 | tf_op jit(solution)/shard_map/all_to_all | solution.py:289
  147.1 0.6 copy.164
  147.7 8.5 %all-to-all-done.2 = bf16[32,9,128]{2,1,0:T(8,128)(2,1)S(1)} async-done(((bf16[32,9,128]{2,1,0:T(8,128)(2,1)}), bf16[32,9,128]{2,1,0:T(8,128)(2,1)S(1)}, u32[]{:S(2)}, u32[]{:S(2)}) %all-to-all-start.2) | async-done | bytes 73760 | tf_op jit(solution)/shard_map/all_to_all | solution.py:289
  156.1 3.9 %all-to-all-start.4 = ((bf16[32,9,2]{1,2,0:T(2,128)(2,1)}), bf16[32,9,2]{1,2,0:T(2,128)(2,1)S(1)}, u32[]{:S(2)}, u32[]{:S(2)}) async-start(bf16[32,9,2]{1,2,0:T(2,128)(2,1)} %copy.164), calls=%async_computation.4 | async-start | bytes 32768 | tf_op jit(solution)/shard_map/all_to_all | solution.py:290
  160.0 8.5 %all-to-all-done.4 = bf16[32,9,2]{1,2,0:T(2,128)(2,1)S(1)} async-done(((bf16[32,9,2]{1,2,0:T(2,128)(2,1)}), bf16[32,9,2]{1,2,0:T(2,128)(2,1)S(1)}, u32[]{:S(2)}, u32[]{:S(2)}) %all-to-all-start.4) | async-done | bytes 1184 | tf_op jit(solution)/shard_map/all_to_all | solution.py:290
  168.5 1.2 broadcast_in_dim.65
  169.7 6.7 %all-to-all-start.3 = ((bf16[16,32,9,128]{3,1,2,0:T(8,128)(2,1)}), bf16[16,32,9,128]{3,1,2,0:T(8,128)(2,1)S(1)}, u32[]{:S(2)}, u32[]{:S(2)}) async-start(bf16[16,32,9,128]{3,1,2,0:T(8,128)(2,1)} %broadcast_in_dim.65), calls=%async_computation.3 | async-start | bytes 2359296 | tf_op jit(solution)/shard_map/all_to_all | solution.py:18
  176.7 30.4 %all-to-all-done.3 = bf16[16,32,9,128]{3,1,2,0:T(8,128)(2,1)S(1)} async-done(((bf16[16,32,9,128]{3,1,2,0:T(8,128)(2,1)}), bf16[16,32,9,128]{3,1,2,0:T(8,128)(2,1)S(1)}, u32[]{:S(2)}, u32[]{:S(2)}) %all-to-all-start.3) | async-done | bytes 1179680 | tf_op jit(solution)/shard_map/all_to_all | solution.py:18
  208.8 1.2 fusion.27
  210.0 2.8 %fusion.71 = f32[288,2048]{1,0:T(8,128)} fusion(bf16[32,2048]{1,0:T(8,128)(2,1)S(1)} %copy-done.2, bf16[2048,32]{0,1:T(8,128)(2,1)S(1)} %copy-done.3, bf16[36,8,16,128]{3,2,1,0:T(8,128)(2,1)S(1)} %bitcast.411, f32[288,32]{0,1:T(8,128)S(1)} %fusion.23, f32[288]{0:T(512)S(1)} %mul.494), kind=kOutput, calls=%fused_computation.89 | convolution fusion | flops 75561984 | bytes 3839104 | tf_op jit(solution)/shard_map/dot_general | solution.py:308
  212.8 3.5 %fusion.19 = bf16[36,8,16,128]{3,1,2,0:T(8,128)(2,1)S(1)} fusion(f32[288,2048]{1,0:T(8,128)} %fusion.71, bf16[1,256,2048]{2,1,0:T(8,128)(2,1)S(1)} %copy-done, bf16[1,2048,256]{2,1,0:T(8,128)(2,1)} %param.38, bf16[36,8,16,128]{3,2,1,0:T(8,128)(2,1)S(1)} %bitcast.412, f32[288,256]{1,0:T(8,128)} %fusion.27, f32[288]{0:T(512)S(1)} %mul.489), kind=kOutput, calls=%fused_computation.29 | convolution fusion | flops 605675520 | bytes 7111808 | tf_op jit(solution)/shard_map/dot_general | solution.py:305
  216.9 34.8 %all_to_all.42 = bf16[16,32,9,128]{3,1,2,0:T(8,128)(2,1)S(1)} all-to-all(bf16[16,32,9,128]{3,1,2,0:T(8,128)(2,1)S(1)} %bitcast.415), channel_id=1, replica_groups=mesh['sp_0'=8,'sp_1'=4,'tp'=16] {'tp'}, dimensions={0} | all-to-all | bytes 2359296 | tf_op jit(solution)/shard_map/all_to_all | solution.py:90
  251.9 0.7 copy.166
  252.6 3.9 %all-to-all-start.6 = ((bf16[32,9,128]{2,1,0:T(8,128)(2,1)}), bf16[32,9,128]{2,1,0:T(8,128)(2,1)S(1)}, u32[]{:S(2)}, u32[]{:S(2)}) async-start(bf16[32,9,128]{2,1,0:T(8,128)(2,1)} %copy.166), calls=%async_computation.6 | async-start | bytes 262144 | tf_op jit(solution)/shard_map/all_to_all | solution.py:314
  256.4 9.9 %all-to-all-done.6 = bf16[32,9,128]{2,1,0:T(8,128)(2,1)S(1)} async-done(((bf16[32,9,128]{2,1,0:T(8,128)(2,1)}), bf16[32,9,128]{2,1,0:T(8,128)(2,1)S(1)}, u32[]{:S(2)}, u32[]{:S(2)}) %all-to-all-start.6) | async-done | bytes 73760 | tf_op jit(solution)/shard_map/all_to_all | solution.py:314
  266.4 0.9 gather_fusion.2
  267.6 11.3 %all_to_all.43 = f32[16,1,256]{2,1,0:T(1,128)S(1)} all-to-all(f32[16,1,256]{2,1,0:T(1,128)S(1)} %broadcast_in_dim.70), channel_id=1, replica_groups=mesh['sp_0'=8,'sp_1'=4,'tp'=16] {'tp'}, dimensions={0} | all-to-all | bytes 32768 | tf_op jit(solution)/shard_map/all_to_all | solution.py:18
  278.9 0.7 multiply_convert_fusion
  (149 shorter events, 14.4 us)
Async XLA Ops:
  0.0 212.8 %copy-start = (bf16[1,256,2048]{2,1,0:T(8,128)(2,1)S(1)}, bf16[1,256,2048]{2,1,0:T(8,128)(2,1)}, u32[]{:S(2)}) copy-start(bf16[1,256,2048]{2,1,0:T(8,128)(2,1)} %param.39) | copy-start | bytes 3145732
  1.8 9.8 %copy-start.6 = (bf16[128,128]{1,0:T(8,128)(2,1)S(1)}, bf16[128,128]{1,0:T(8,128)(2,1)}, u32[]{:S(2)}) copy-start(bf16[128,128]{1,0:T(8,128)(2,1)} %param.25) | copy-start | bytes 98308
  69.9 22.7 %copy-start.5 = (bf16[128,128]{1,0:T(8,128)(2,1)S(1)}, bf16[128,128]{1,0:T(8,128)(2,1)}, u32[]{:S(2)}) copy-start(bf16[128,128]{1,0:T(8,128)(2,1)} %param.31) | copy-start | bytes 98308
  76.8 16.0 %copy-start.1 = (bf16[128,2048]{1,0:T(8,128)(2,1)S(1)}, bf16[128,2048]{1,0:T(8,128)(2,1)}, u32[]{:S(2)}) copy-start(bf16[128,2048]{1,0:T(8,128)(2,1)} %param.32) | copy-start | bytes 1572868
  93.1 17.1 %copy-start.7 = (s32[128,2]{0,1:T(2,128)S(1)}, s32[128,2]{0,1:T(2,128)}, u32[]{:S(2)}) copy-start(s32[128,2]{0,1:T(2,128)} %param.35) | copy-start | bytes 3076
  93.1 18.6 %copy-start.8 = (bf16[128,2]{0,1:T(2,128)(2,1)S(1)}, bf16[128,2]{0,1:T(2,128)(2,1)}, u32[]{:S(2)}) copy-start(bf16[128,2]{0,1:T(2,128)(2,1)} %param.36) | copy-start | bytes 1540
  94.0 33.3 %all-to-all-start = ((bf16[16,128,128]{2,1,0:T(8,128)(2,1)}), bf16[16,128,128]{2,1,0:T(8,128)(2,1)S(1)}, u32[]{:S(2)}, u32[]{:S(2)}) async-start(bf16[16,128,128]{2,1,0:T(8,128)(2,1)} %bitcast.376), calls=%async_computation | async-start | bytes 1048576 | tf_op jit(solution)/shard_map/all_to_all | solution.py:90
  110.2 17.3 %copy-start.4 = (bf16[128,128]{1,0:T(8,128)(2,1)S(1)}, bf16[128,128]{1,0:T(8,128)(2,1)}, u32[]{:S(2)}) copy-start(bf16[128,128]{1,0:T(8,128)(2,1)} %param.33) | copy-start | bytes 98308
  110.3 28.3 %copy-start.9 = (f32[128]{0:T(128)S(1)}, f32[128]{0:T(128)}, u32[]{:S(2)}) copy-start(f32[128]{0:T(128)} %param.34) | copy-start | bytes 1540
  128.2 10.3 %all-to-all-start.1 = ((f32[16,1,256]{2,1,0:T(1,128)}), f32[16,1,256]{2,1,0:T(1,128)S(1)}, u32[]{:S(2)}, u32[]{:S(2)}) async-start(f32[16,1,256]{2,1,0:T(1,128)} %broadcast_in_dim.56), calls=%async_computation.1 | async-start | bytes 32768 | tf_op jit(solution)/shard_map/all_to_all | solution.py:18
  140.9 15.2 %all-to-all-start.2 = ((bf16[32,9,128]{2,1,0:T(8,128)(2,1)}), bf16[32,9,128]{2,1,0:T(8,128)(2,1)S(1)}, u32[]{:S(2)}, u32[]{:S(2)}) async-start(bf16[32,9,128]{2,1,0:T(8,128)(2,1)} %broadcast_select_fusion), calls=%async_computation.2 | async-start | bytes 262144 | tf_op jit(solution)/shard_map/all_to_all | solution.py:289
  156.1 12.4 %all-to-all-start.4 = ((bf16[32,9,2]{1,2,0:T(2,128)(2,1)}), bf16[32,9,2]{1,2,0:T(2,128)(2,1)S(1)}, u32[]{:S(2)}, u32[]{:S(2)}) async-start(bf16[32,9,2]{1,2,0:T(2,128)(2,1)} %copy.164), calls=%async_computation.4 | async-start | bytes 32768 | tf_op jit(solution)/shard_map/all_to_all | solution.py:290
  169.7 37.4 %all-to-all-start.3 = ((bf16[16,32,9,128]{3,1,2,0:T(8,128)(2,1)}), bf16[16,32,9,128]{3,1,2,0:T(8,128)(2,1)S(1)}, u32[]{:S(2)}, u32[]{:S(2)}) async-start(bf16[16,32,9,128]{3,1,2,0:T(8,128)(2,1)} %broadcast_in_dim.65), calls=%async_computation.3 | async-start | bytes 2359296 | tf_op jit(solution)/shard_map/all_to_all | solution.py:18
  207.1 0.9 copy-start.12
  207.6 1.2 copy-start.11
  208.8 1.2 copy-start.2
  208.8 1.2 copy-start.3
  251.7 27.2 %copy-start.10 = (f32[128]{0:T(128)S(1)}, f32[128]{0:T(128)}, u32[]{:S(2)}) copy-start(f32[128]{0:T(128)} %param.43) | copy-start | bytes 1540
  252.6 13.8 %all-to-all-start.6 = ((bf16[32,9,128]{2,1,0:T(8,128)(2,1)}), bf16[32,9,128]{2,1,0:T(8,128)(2,1)S(1)}, u32[]{:S(2)}, u32[]{:S(2)}) async-start(bf16[32,9,128]{2,1,0:T(8,128)(2,1)} %copy.166), calls=%async_computation.6 | async-start | bytes 262144 | tf_op jit(solution)/shard_map/all_to_all | solution.py:314
where the time goes:
time: 281 us; the launch traced here: 280 us
  blocking collectives  83.3 us (30%)
  waiting for transfers between devices  75.4 us (27%)
  starting transfers between devices  39.8 us (14%)
  between operations  34.2 us (12%)
  local copies, waits for them, and re-layouts  19.8 us (7%)
  matrix products  15.6 us (6%)
  other arithmetic  11.5 us (4%)
    all_gather x2, blocking collectives, collected_together(): both, at, found = (lax.all_gather(jnp.concatenate(lines), axis), 0, {})  37.2 us
    all_to_all x2, waiting for transfers between devices, sent_to_all(): lax.all_to_all(jnp.broadcast_to(value[None], (peers, *value.shape)), axis...  37.1 us
    all_to_all x1, blocking collectives, sent_and_summed(): lax.all_to_all(pieces, axis, split_axis=0, concat_axis=0, tiled=True)  34.8 us
    all_to_all x1, starting transfers between devices, sent_and_summed(): lax.all_to_all(pieces, axis, split_axis=0, concat_axis=0, tiled=True)  16.1 us
    all_to_all x1, waiting for transfers between devices, sent_and_summed(): lax.all_to_all(pieces, axis, split_axis=0, concat_axis=0, tiled=True)  11.4 us
    all_to_all x1, blocking collectives, sent_to_all(): lax.all_to_all(jnp.broadcast_to(value[None], (peers, *value.shape)), axis...  11.3 us
    all_to_all x2, starting transfers between devices, sent_to_all(): lax.all_to_all(jnp.broadcast_to(value[None], (peers, *value.shape)), axis...  10.1 us
    all_to_all x1, waiting for transfers between devices, shards(): lax.all_to_all(summed, SP, split_axis=0, concat_axis=0, tiled=True)  9.9 us
  transfers between devices with their start and end apart: 6, of which 6 were waited for; matrix products, arithmetic and copies ran while one was open for 2% of the time, Pallas kernels for 0%

commit v1 on v0

v1 whole, which is shorter than its diff:
```python
import functools

import jax
import jax.numpy as jnp
from jax import lax
from jax.experimental import pallas as pl
from jax.experimental.pallas import tpu as pltpu
from jax.sharding import PartitionSpec as P

BLOCK = 64
ALPHA = 2.0**0.25
F32 = jnp.float32
BF16 = jnp.bfloat16
MESH = pl.DeviceIdType.MESH
REACH = 3


def iota(shape, dim):
    return lax.broadcasted_iota(jnp.int32, shape, dim)


def mm(a, b):
    return jnp.dot(a.astype(BF16), b.astype(BF16), preferred_element_type=F32)


def mm_nt(a, b):
    return lax.dot_general(
        a.astype(BF16), b.astype(BF16), (((1,), (1,)), ((), ())), preferred_element_type=F32
    )


def mm_tn(a, b):
    return lax.dot_general(
        a.astype(BF16), b.astype(BF16), (((0,), (0,)), ((), ())), preferred_element_type=F32
    )


def silu(v):
    return v / (1.0 + jnp.exp(-v))


def kernel(dims, *refs):
    n_sp, n_tp, rows, experts, cap, stride = dims
    ny = n_tp // 2
    slots = n_sp * cap
    padded = n_sp * stride
    names = dims_names()
    hbm = dict(zip(names, refs[: len(names)]))
    chan_ref, out_hbm = refs[len(names)], refs[len(names) + 1]
    scratch = refs[len(names) + 2 :]
    vm = dict(zip(names, scratch[: len(names)]))
    (
        prev_label, pay, pieces, carry_out, carry_in,
        part1, pair1, send1, recv1,
        stat1, stat2,
        sent, arrived, gathered, acc_g, acc_s,
        part2, pair2, send2, recv2,
        rsend, returned, out_vm,
        load_sem, out_sem, lab_sem, pa_s, pa_r, pb_s,
        d1_s, d1_r, y1_s, y1_r, st1_s, st1_r,
        dis_s, dis_r, big_s, big_r, small_s, small_r, own_s, own_r,
        d2_s, d2_r, y2_s, y2_r, ret_s, ret_r, st2_s, st2_r,
    ) = scratch[len(names) :]

    s = lax.axis_index("sp")
    t = lax.axis_index("tp")
    y = t // 2
    c = lax.rem(t, 2)
    other = 1 - c

    def at_sp(k):
        return {"sp": k, "tp": t}

    def at_tp(k):
        return {"sp": s, "tp": k}

    def remote(src, dst, send_sem, recv_sem, device):
        return pltpu.make_async_remote_copy(
            src_ref=src, dst_ref=dst, send_sem=send_sem, recv_sem=recv_sem,
            device_id=device, device_id_type=MESH,
        )

    loads = {
        name: pltpu.make_async_copy(hbm[name], vm[name], load_sem.at[k])
        for k, name in enumerate(names)
    }
    for name in names:
        loads[name].start()
    barrier = pltpu.get_barrier_semaphore()

    def greet_sp(k, carry):
        pl.semaphore_signal(
            barrier, inc=1, device_id=at_sp(lax.rem(s + k, n_sp)), device_id_type=MESH
        )
        return carry

    def greet_tp(k, carry):
        pl.semaphore_signal(
            barrier, inc=1, device_id=at_tp(lax.rem(t + k, n_tp)), device_id_type=MESH
        )
        return carry

    lax.fori_loop(1, n_sp, greet_sp, 0)
    lax.fori_loop(1, n_tp, greet_tp, 0)

    for name in ("probe", "address", "content", "storage", "fade", "extra", "label"):
        loads[name].wait()
    pl.semaphore_wait(barrier, n_sp + n_tp - 2)
    lab_copy = remote(
        vm["label"], prev_label, lab_sem.at[0], lab_sem.at[1], at_sp(lax.rem(s + 1, n_sp))
    )
    lab_copy.start()

    row_i, col_i = iota((rows, rows), 0), iota((rows, rows), 1)
    eye = row_i == col_i
    lower, strict = row_i >= col_i, row_i > col_i
    same_block = (row_i < BLOCK) == (col_i < BLOCK)

    def to_col(row):
        return jnp.sum(jnp.where(eye, row, 0.0), axis=1, keepdims=True)

    def to_row(col):
        return jnp.sum(jnp.where(eye, col, 0.0), axis=0, keepdims=True)

    queries = vm["probe"][...].astype(F32)
    keys = vm["address"][...].astype(F32)
    values = vm["content"][...].astype(F32)
    q_unit = queries * lax.rsqrt(
        jnp.sum(queries * queries, -1, keepdims=True) + 1e-06
    ) * queries.shape[-1] ** (-0.5)
    k_unit = keys * lax.rsqrt(jnp.sum(keys * keys, -1, keepdims=True) + 1e-06)
    gate = to_col(1.0 / (1.0 + jnp.exp(-vm["storage"][...])))
    fade = vm["fade"][...]
    softplus = jnp.maximum(fade, 0.0) + jnp.log(1.0 + jnp.exp(-jnp.abs(fade)))
    rate = jnp.exp(jnp.full(fade.shape, chan_ref[0], F32))
    decay = vm["extra"][...] - rate * softplus
    c_col = jnp.sum(jnp.where(lower, decay, 0.0), axis=1, keepdims=True)
    c_row = to_row(c_col)
    label_row = vm["label"][...].astype(F32)
    label_col = to_col(label_row)
    label_first, label_last = label_row[:, :1], label_row[:, rows - 1 :]
    c_last = c_row[:, rows - 1 :]
    reach = jnp.where(
        lower & (label_col == label_row), jnp.exp(jnp.where(lower, c_col - c_row, 0.0)), 0.0
    )
    weighted = k_unit * gate
    coupling = jnp.where(strict, mm_nt(weighted, k_unit) * reach, 0.0)
    power = jnp.where(same_block, coupling, 0.0)
    across = jnp.where(same_block, 0.0, coupling)
    inverse = jnp.where(eye, 1.0, 0.0) - power
    for _ in range(BLOCK.bit_length() - 2):
        power = mm(power, power)
        inverse = inverse + mm(inverse, power)
    inverse = inverse - mm(inverse, mm(across, inverse))
    growth = jnp.exp(c_col) * (label_col == label_first).astype(F32)
    both = mm(inverse, jnp.concatenate([weighted * growth, values * gate], axis=1))
    tail_keys = k_unit * (jnp.exp(c_last - c_col) * (label_col == label_last).astype(F32))
    ends = mm_tn(tail_keys, both)
    end_growth = jnp.exp(c_last) * (label_last == label_first).astype(F32)
    scores = mm_nt(q_unit, k_unit) * reach
    outs = mm(scores, both)
    width = q_unit.shape[-1]
    q_grown = q_unit * growth - outs[:, :width]
    own_mixed = outs[:, width:]
    lab_copy.wait()
    joined = (label_first == prev_label[...].astype(F32)[:, rows - 1 :]).astype(F32)
    state_map = (jnp.where(eye, end_growth, 0.0) - ends[:, :width]) * joined
    pay[0:width, :] = state_map.astype(BF16)
    pay[width:, :] = ends[:, width:].astype(BF16)
    first = [
        remote(pay, pieces.at[k], pa_s.at[k], pa_r.at[k], at_sp(lax.rem(s + k + 1, n_sp)))
        for k in range(REACH)
    ]
    for k in reversed(range(REACH)):
        first[k].start()

    for name in names:
        if name not in ("probe", "address", "content", "storage", "fade", "extra", "label"):
            loads[name].wait()
    pick0, pick1 = vm["picks"][0:1, :], vm["picks"][1:2, :]
    share = vm["share"][...].astype(F32)
    expert_i = iota((experts, rows), 0)
    to0, to1 = (expert_i == pick0).astype(F32), (expert_i == pick1).astype(F32)
    chosen = to0 + to1
    rank = mm(chosen, (row_i < col_i).astype(F32))
    coded = jnp.where(chosen > 0.0, rank + 1.0, 0.0)
    shares = to0 * share[0:1, :] + to1 * share[1:2, :]
    slot_i = iota((padded, experts), 0)
    from_e = iota((padded, experts), 1) * stride
    spread = ((slot_i >= from_e) & (slot_i < from_e + stride)).astype(F32)
    place = iota((n_sp, stride, rows), 1).reshape(padded, rows)
    wide = mm(spread, jnp.concatenate([coded, shares, to0], axis=1))
    hot = wide[:, :rows] == (place + 1).astype(F32)
    dispatch = hot.astype(BF16)
    slot_share = jnp.sum(jnp.where(hot, wide[:, rows : 2 * rows], 0.0), axis=1, keepdims=True)
    slot_first = jnp.sum(jnp.where(hot, wide[:, 2 * rows :], 0.0), axis=1, keepdims=True)
    lane = iota((padded, rows), 1)
    here = (lane == place).astype(F32)
    told = mm_tn(spread, jnp.concatenate([here * slot_share, here * slot_first], axis=1))
    told = mm(spread, told)
    notes = jnp.where(place == cap, told[:, :rows], 0.0) + jnp.where(
        place == cap + 1, told[:, rows:], 0.0
    )
    compact_i = iota((slots, padded), 0).astype(F32)
    source = jnp.floor((compact_i + 0.5) * (1.0 / cap))
    within = compact_i - source * cap
    column = iota((slots, padded), 1).astype(F32)
    compact = (column == source * stride + within).astype(BF16)
    note_row = (column == source * stride + cap).astype(BF16)
    flag_row = (column == source * stride + cap + 1).astype(BF16)
    slot_lane = iota((slots, rows), 1).astype(F32) == within[:, :rows]

    for k in range(REACH):
        first[k].wait_recv()
    map1, shift1 = pieces[0, 0:width, :], pieces[0, width:, :].astype(F32)
    map2, shift2 = pieces[1, 0:width, :], pieces[1, width:, :].astype(F32)
    map3, shift3 = pieces[2, 0:width, :], pieces[2, width:, :]
    shift23 = shift2 + mm(map2, shift3)
    shift123 = shift1 + mm(map1, shift23)
    carry_out[...] = shift123.astype(BF16)
    second = remote(
        carry_out, carry_in, pb_s.at[0], pb_s.at[1], at_sp(lax.rem(s + REACH, n_sp))
    )
    second.start()
    map123 = mm(mm(map1, map2), map3)
    valve = silu(vm["exit"][...].astype(F32))
    second.wait_recv()
    incoming = (shift123 + mm(map123, carry_in[...])) * joined
    mixed = own_mixed + mm(q_grown, incoming)
    scaled = mixed * lax.rsqrt(jnp.mean(mixed * mixed, -1, keepdims=True) + 1e-06)
    heads_out = (scaled * valve).astype(BF16)

    far_first = sorted(range(1, ny), key=lambda k: -min(k, ny - k))

    def scattered_sum(part, pair, send, recv, d_s, d_r, y_s, y_r):
        near = {}
        for k in far_first + [0]:
            chip = lax.rem(y + k, ny)
            near[k] = remote(
                part.at[chip, other], pair.at[chip], d_s.at[k], d_r.at[k], at_tp(2 * y + other)
            )
            near[k].start()
        far = {}
        for k in far_first:
            chip = lax.rem(y + k, ny)
            near[k].wait_recv()
            send[chip] = (part[chip, c].astype(F32) + pair[chip].astype(F32)).astype(BF16)
            far[k] = remote(send.at[chip], recv.at[y], y_s.at[k], y_r.at[k], at_tp(2 * chip + c))
            far[k].start()
        near[0].wait_recv()
        total = part[y, c].astype(F32) + pair[y].astype(F32)
        for k in reversed(far_first):
            far[k].wait_recv()
            total = total + recv[lax.rem(y - k + ny, ny)].astype(F32)
        for k in near:
            near[k].wait_send()
        for k in far:
            far[k].wait_send()
        return total

    for chip in range(ny):
        product = mm(heads_out, vm["final"][:, chip * 2 * width : (chip + 1) * 2 * width])
        part1[chip, 0] = product[:, :width].astype(BF16)
        part1[chip, 1] = product[:, width:].astype(BF16)
    projected = scattered_sum(part1, pair1, send1, recv1, d1_s, d1_r, y1_s, y1_r)

    def normed(summed, gain, stat, s_sem, r_sem):
        features = summed.shape[-1] * n_tp
        stat[t, 0:1, :] = to_row(jnp.sum(summed, -1, keepdims=True))
        stat[t, 1:2, :] = to_row(jnp.sum(summed * summed, -1, keepdims=True))
        told = [
            remote(
                stat.at[t], stat.at[t], s_sem.at[k], r_sem.at[k], at_tp(lax.rem(t + k, n_tp))
            )
            for k in range(1, n_tp)
        ]
        for copy in told:
            copy.start()
        for copy in told:
            copy.wait()
        totals = jnp.sum(stat[...], axis=0)
        mean = totals[0:1, :] / features
        var = totals[1:2, :] / features - mean * mean
        scale = lax.rsqrt(var + 1e-05)
        return (summed - to_col(mean)) * to_col(scale) * gain

    first_sum = ALPHA * vm["incoming"][...].astype(F32) + projected
    middle = normed(first_sum, vm["gain1"][...], stat1, st1_s, st1_r).astype(BF16)

    def exchange(src, dst, s_sem, r_sem):
        def copy(k):
            to = lax.rem(s + k, n_sp)
            return remote(src.at[to], dst.at[s], s_sem.at[k], r_sem.at[k], at_sp(to))

        def start(k, carry):
            copy(k).start()
            return carry

        def finish(k, carry):
            copy(k).wait()
            return carry

        lax.fori_loop(1, n_sp, start, 0)
        dst[s] = src[s]
        lax.fori_loop(1, n_sp, finish, 0)
        return dst[...].reshape(padded, -1)

    payload = jnp.dot(dispatch, middle, preferred_element_type=F32) + notes
    sent[...] = payload.astype(BF16).reshape(n_sp, stride, rows)
    came = exchange(sent, arrived, dis_s, dis_r)
    own_rows = jnp.dot(compact, came, preferred_element_type=F32).astype(BF16)

    lanes = pl.ds(pl.multiple_of(c * width, width), width)
    ahead = lax.rem(y + 1 - 2 * c + ny, ny)
    behind = lax.rem(y - 1 + 2 * c + ny, ny)
    most, least = ny // 2, (ny - 1) // 2

    def origin(k):
        return lax.rem(y - k * (1 - 2 * c) + 2 * ny, ny)

    gathered[y, :, lanes] = own_rows

    def block(chip):
        return gathered.at[chip, :, lanes]

    def hand(k, chip):
        return remote(block(chip), block(chip), own_s.at[k], own_r.at[k], at_tp(2 * y + other))

    def big(k):
        chip = origin(k)
        return remote(block(chip), block(chip), big_s.at[k], big_r.at[k], at_tp(2 * ahead + c))

    def small(k):
        chip = origin(-k)
        return remote(
            block(chip), block(chip), small_s.at[k], small_r.at[k], at_tp(2 * behind + c)
        )

    def big_wait(k):
        chip = origin(k + 1)
        remote(
            block(chip), block(chip), big_s.at[k], big_r.at[k], at_tp(2 * ahead + c)
        ).wait_recv()

    def small_wait(k):
        chip = origin(-k - 1)
        remote(
            block(chip), block(chip), small_s.at[k], small_r.at[k], at_tp(2 * behind + c)
        ).wait_recv()

    def hand_wait(k, chip):
        other_lanes = pl.ds(pl.multiple_of(other * width, width), width)
        there = gathered.at[chip, :, other_lanes]
        remote(there, there, own_s.at[k], own_r.at[k], at_tp(2 * y + other)).wait_recv()

    def absorb(chip, fresh):
        block_in = gathered[chip]
        at = pl.ds(pl.multiple_of(chip * 2 * width, 2 * width), 2 * width)
        gates = jnp.dot(block_in, vm["valve"][at, :], preferred_element_type=F32)
        ups = jnp.dot(block_in, vm["raise"][at, :], preferred_element_type=F32)
        common = lax.dot_general(
            block_in, vm["common"][:, at], (((1,), (1,)), ((), ())), preferred_element_type=F32
        )
        if fresh:
            acc_g[0], acc_g[1], acc_s[...] = gates, ups, common
        else:
            acc_g[0] += gates
            acc_g[1] += ups
            acc_s[...] += common

    big(0).start()
    if least:
        small(0).start()
    hand(0, y).start()
    share_rows = jnp.dot(note_row, came, preferred_element_type=F32)
    slot_weight = jnp.sum(jnp.where(slot_lane, share_rows, 0.0), axis=1, keepdims=True)
    flag_rows = jnp.dot(flag_row, came, preferred_element_type=F32)
    slot_flag = jnp.sum(jnp.where(slot_lane, flag_rows, 0.0), axis=1, keepdims=True)
    hand_wait(0, y)
    absorb(y, True)
    for k in range(1, most + 1):
        big_wait(k - 1)
        if k < most:
            big(k).start()
        hand(2 * k - 1, origin(k)).start()
        if k <= least:
            small_wait(k - 1)
            if k < least:
                small(k).start()
            hand(2 * k, origin(-k)).start()
        hand_wait(2 * k - 1, origin(-k))
        absorb(origin(-k), False)
        if k <= least:
            hand_wait(2 * k, origin(k))
            absorb(origin(k), False)

    hidden = (silu(acc_g[0]) * acc_g[1] * slot_weight).astype(BF16)
    sf = acc_s.shape[1] // 2
    common = acc_s[...]
    shared = (silu(common[:, :sf]) * common[:, sf:] * slot_flag).astype(BF16)
    for chip in range(ny):
        at = slice(chip * 2 * width, (chip + 1) * 2 * width)
        product = jnp.dot(hidden, vm["lower"][:, at], preferred_element_type=F32) + jnp.dot(
            shared, vm["common_low"][:, at], preferred_element_type=F32
        )
        part2[chip, 0] = product[:, :width].astype(BF16)
        part2[chip, 1] = product[:, width:].astype(BF16)
    summed = scattered_sum(part2, pair2, send2, recv2, d2_s, d2_r, y2_s, y2_r)

    rsend[...] = mm_tn(compact, summed).astype(BF16).reshape(n_sp, stride, rows)
    back = exchange(rsend, returned, ret_s, ret_r)
    mixture = mm_tn(dispatch, back)
    second_sum = ALPHA * middle.astype(F32) + mixture
    out_vm[...] = normed(second_sum, vm["gain2"][...], stat2, st2_s, st2_r).astype(BF16)
    out_copy = pltpu.make_async_copy(out_vm, out_hbm, out_sem)
    out_copy.start()

    for copy in first:
        copy.wait_send()
    second.wait_send()
    for k in range(most):
        big(k).wait_send()
        hand(2 * k + 1, origin(k + 1)).wait_send()
    for k in range(least):
        small(k).wait_send()
        hand(2 * k + 2, origin(-k - 1)).wait_send()
    hand(0, y).wait_send()
    out_copy.wait()


def dims_names():
    return (
        "probe", "address", "content", "storage", "fade", "extra", "label",
        "picks", "share", "exit", "incoming", "gain1", "gain2", "final",
        "valve", "raise", "lower", "common", "common_low",
    )


def shards(
    probe, address, content, storage, fade, channel, extra, label, exit_valve, final,
    incoming, gain1, picks, share, valve, raising, lowering, common_valve, common_raising,
    common_lowering, gain2,
):
    n_sp, n_tp = lax.axis_size("sp"), lax.axis_size("tp")
    ny = n_tp // 2
    rows, width = probe.shape
    experts = n_sp * valve.shape[0]
    cap = max(2, 9 * rows * picks.shape[1] // (8 * experts))
    stride = -(-(cap + 2) // 16) * 16
    slots = n_sp * cap
    ff, features = valve.shape[2], valve.shape[1]
    sf = common_valve.shape[1]
    dims = (n_sp, n_tp, rows, experts, cap, stride)
    args = {
        "probe": probe, "address": address, "content": content, "storage": storage,
        "fade": fade, "extra": extra, "label": label[None, :], "picks": picks.T,
        "share": share.T, "exit": exit_valve, "incoming": incoming, "gain1": gain1[None, :],
        "gain2": gain2[None, :], "final": final, "valve": valve[0], "raise": raising[0],
        "lower": lowering[0],
        "common": jnp.concatenate([common_valve.T, common_raising.T], axis=0),
        "common_low": common_lowering,
    }
    names = dims_names()
    operands = [args[n] for n in names]
    dma = pltpu.SemaphoreType.DMA
    own = [pltpu.VMEM(a.shape, a.dtype) for a in operands]

    def vmem(*shape, kind=BF16):
        return pltpu.VMEM(shape, kind)

    return pl.pallas_call(
        functools.partial(kernel, dims),
        out_shape=jax.ShapeDtypeStruct((rows, width), BF16),
        in_specs=[pl.BlockSpec(memory_space=pl.ANY)] * len(operands)
        + [pl.BlockSpec(memory_space=pltpu.SMEM)],
        out_specs=pl.BlockSpec(memory_space=pl.ANY),
        scratch_shapes=own
        + [
            vmem(1, rows, kind=jnp.int32), vmem(2 * width, width), vmem(REACH, 2 * width, width),
            vmem(width, width), vmem(width, width),
            vmem(ny, 2, rows, width), vmem(ny, rows, width), vmem(ny, rows, width),
            vmem(ny, rows, width),
            vmem(n_tp, 2, rows, kind=F32), vmem(n_tp, 2, rows, kind=F32),
            vmem(n_sp, stride, width), vmem(n_sp, stride, width),
            vmem(ny, slots, 2 * width), vmem(2, slots, ff, kind=F32), vmem(slots, 2 * sf, kind=F32),
            vmem(ny, 2, slots, width), vmem(ny, slots, width), vmem(ny, slots, width),
            vmem(ny, slots, width),
            vmem(n_sp, stride, width), vmem(n_sp, stride, width), vmem(rows, width),
            dma((len(operands),)), dma, dma((2,)), dma((REACH,)), dma((REACH,)), dma((2,)),
            dma((ny,)), dma((ny,)), dma((ny,)), dma((ny,)), dma((n_tp,)), dma((n_tp,)),
            dma((n_sp,)), dma((n_sp,)), dma((ny,)), dma((ny,)), dma((ny,)), dma((ny,)),
            dma((ny,)), dma((ny,)),
            dma((ny,)), dma((ny,)), dma((ny,)), dma((ny,)), dma((n_sp,)), dma((n_sp,)),
            dma((n_tp,)), dma((n_tp,)),
        ],
        compiler_params=pltpu.CompilerParams(
            collective_id=0, has_side_effects=True, vmem_limit_bytes=60 * 1024 * 1024
        ),
        name="layer",
    )(*operands, channel)


def solution(mesh):
    return jax.shard_map(
        shards,
        mesh=mesh,
        in_specs=(
            P("sp", "tp"), P("sp", "tp"), P("sp", "tp"), P("tp", "sp"), P("tp", "sp"), P("tp"),
            P("tp", "sp"), P("sp"), P("sp", "tp"), P("tp", None), P("sp", "tp"), P("tp"),
            P("sp", None), P("sp", None), P("sp", None, "tp"), P("sp", None, "tp"),
            P("sp", "tp", None), P(None, "tp"), P(None, "tp"), P("tp", None), P("tp"),
        ),
        out_specs=P("sp", "tp"),
        check_vma=False,
    )
```

time: 281 us -> 104 us (0.37)
  Pallas kernels: 0 us -> 99.6 us
  blocking collectives: 83.3 us -> 0 us
  waiting for transfers between devices: 75.4 us -> 0 us
  starting transfers between devices: 39.8 us -> 0 us
  between operations: 34.2 us -> 0.66 us
  local copies, waits for them, and re-layouts: 19.8 us -> 1.38 us
  matrix products: 15.6 us -> 0 us
  other arithmetic: 11.5 us -> 1.68 us
    pallas_call x0 -> x1, Pallas kernels: none -> 99.6 us  [shards(): pl.pallas_call(functools.partial(kernel, dims), out_shape=jax.ShapeDtypeS...]
    all_to_all x6 -> x0, waiting for transfers between devices: 75.4 us -> none  [the longest x2 37.1 us: sent_to_all(): lax.all_to_all(jnp.broadcast_to(value[None], (peers, *value.shape)), axis...]
    all_to_all x2 -> x0, blocking collectives: 46.1 us -> none  [the longest x1 34.8 us: sent_and_summed(): lax.all_to_all(pieces, axis, split_axis=0, concat_axis=0, tiled=True)]
    all_to_all x6 -> x0, starting transfers between devices: 39.8 us -> none  [the longest x1 16.1 us: sent_and_summed(): lax.all_to_all(pieces, axis, split_axis=0, concat_axis=0, tiled=True)]
    all_gather x2 -> x0, blocking collectives: 37.2 us -> none  [collected_together(): both, at, found = (lax.all_gather(jnp.concatenate(lines), axis), 0, {})]
    dot_general x42 -> x0, matrix products: 15.6 us -> none  [the longest x37 7.3 us: matmul_high(): return jnp.einsum(form, left, right)]
    gather x4 -> x0, local copies, waits for them, and re-layouts: 4.65 us -> none  [the longest x1 2.37 us: shards(): picked_specialist_share.reshape(picks)[safe_owner]]
    slice x12 -> x0, local copies, waits for them, and re-layouts: 4.07 us -> none  [the longest x4 2.4 us: prefix_by_axis(): part[k].astype(own.dtype)]
  transfers between devices with their start and end apart: 6 -> 0, of which waited for: 6 -> 0; matrix products, arithmetic and copies ran while one was open for 2% -> 0% of each run, Pallas kernels for 0% -> 0%
where the time goes in v1:
time: 104 us; the launch traced here: 103 us
  Pallas kernels  99.6 us (96%)
  other arithmetic  1.68 us (2%)
  local copies, waits for them, and re-layouts  1.38 us (1%)
    pallas_call x1, Pallas kernels, shards(): pl.pallas_call(functools.partial(kernel, dims), out_shape=jax.ShapeDtypeS...  99.6 us

profile of v1, /device:TPU:1, one launch (start us, length us, event | category | flops | bytes accessed | tf_op | source)
XLA Modules:
  0.0 103.3 jit_solution(3857199543934268236)
XLA Ops:
  0.7 1.7 %pad_maximum_fusion.refs_17_ = bf16[64,2048]{1,0:T(8,128)(2,1)} fusion(bf16[32,2048]{1,0:T(8,128)(2,1)} %bitcast.13, bf16[32,2048]{1,0:T(8,128)(2,1)} %bitcast.14), kind=kLoop, calls=%fused_computation | loop fusion | flops 524288 | bytes 524288 | tf_op jit(solution)/shard_map/concatenate | solution.py:460
  2.3 99.6 %layer.1 = bf16[128,128]{1,0:T(8,128)(2,1)} custom-call(bf16[128,128]{1,0:T(8,128)(2,1)} %refs_0_.1, bf16[128,128]{1,0:T(8,128)(2,1)} %refs_1_.1, bf16[128,128]{1,0:T(8,128)(2,1)} %refs_2_.1, f32[1,128]{1,0:T(1,128)} %refs_3_.1, f32[1,128]{1,0:T(1,128)} %refs_4_.1, f32[1,128]{1,0:T(1,128)} %refs_5_.1, s32[1,128]{1,0:T(1,128)} %bitcast.16, ...), custom_call_target="tpu_custom_call" | custom-call | tf_op jit(solution)/shard_map/layer/pallas_call | solution.py:471
  101.9 1.4 %copy.24 = bf16[128,128]{1,0:T(8,128)(2,1)} copy(bf16[128,128]{1,0:T(8,128)(2,1)} %layer.1) | data formatting | bytes 65536

commit v2 on v1

v2 whole, which is shorter than its diff:
```python
import functools

import jax
import jax.numpy as jnp
from jax import lax
from jax.experimental import pallas as pl
from jax.experimental.pallas import tpu as pltpu
from jax.sharding import PartitionSpec as P

BLOCK = 64
ALPHA = 2.0**0.25
F32 = jnp.float32
BF16 = jnp.bfloat16
MESH = pl.DeviceIdType.MESH
REACH = 3


def iota(shape, dim):
    return lax.broadcasted_iota(jnp.int32, shape, dim)


def mm(a, b):
    return jnp.dot(a.astype(BF16), b.astype(BF16), preferred_element_type=F32)


def mm_nt(a, b):
    return lax.dot_general(
        a.astype(BF16), b.astype(BF16), (((1,), (1,)), ((), ())), preferred_element_type=F32
    )


def mm_tn(a, b):
    return lax.dot_general(
        a.astype(BF16), b.astype(BF16), (((0,), (0,)), ((), ())), preferred_element_type=F32
    )


def silu(v):
    return v / (1.0 + jnp.exp(-v))


def kernel(dims, *refs):
    n_sp, n_tp, rows, experts, cap, stride = dims
    ny = n_tp // 2
    slots = n_sp * cap
    padded = n_sp * stride
    names = dims_names()
    hbm = dict(zip(names, refs[: len(names)]))
    out_hbm = refs[len(names)]
    scratch = refs[len(names) + 1 :]
    vm = dict(zip(names, scratch[: len(names)]))
    (
        pay, pieces, carry_out, carry_in,
        part1, pair1, send1, recv1,
        stat0, stat1, stat2,
        sent, arrived, told, heard, gathered, acc_g, acc_s,
        part2, pair2, send2, recv2,
        rsend, returned, out_vm,
        load_sem, out_sem, pa_s, pa_r, pb_s,
        d1_r, y1_r, mean_s, sq1_s, sq2_s,
        dis_s, note_s, ret_s, big_r, small_r, own_r, gone_s,
        d2_r, y2_r,
    ) = scratch[len(names) :]

    s = lax.axis_index("sp")
    t = lax.axis_index("tp")
    y = t // 2
    c = lax.rem(t, 2)
    other = 1 - c

    def at_sp(k):
        return {"sp": k, "tp": t}

    def at_tp(k):
        return {"sp": s, "tp": k}

    def remote(src, dst, send_sem, recv_sem, device):
        return pltpu.make_async_remote_copy(
            src_ref=src, dst_ref=dst, send_sem=send_sem, recv_sem=recv_sem,
            device_id=device, device_id_type=MESH,
        )

    barrier = pltpu.get_barrier_semaphore()

    def greet_sp(k, carry):
        pl.semaphore_signal(
            barrier, inc=1, device_id=at_sp(lax.rem(s + k, n_sp)), device_id_type=MESH
        )
        return carry

    def greet_tp(k, carry):
        pl.semaphore_signal(
            barrier, inc=1, device_id=at_tp(lax.rem(t + k, n_tp)), device_id_type=MESH
        )
        return carry

    lax.fori_loop(1, n_sp, greet_sp, 0)
    lax.fori_loop(1, n_tp, greet_tp, 0)
    sf = vm["common"].shape[0] // 2
    loads = {}
    for k, name in enumerate(names):
        into = vm[name]
        if name == "common":
            into = vm["common"].at[0:sf]
        if name == "common_raise":
            into = vm["common"].at[sf:]
        loads[name] = pltpu.make_async_copy(hbm[name], into, load_sem.at[k])
    early = ("probe", "address", "content", "storage", "fade", "extra", "channel", "label")
    for name in early:
        loads[name].start()
    for name in names:
        if name not in early:
            loads[name].start()
    for name in early:
        loads[name].wait()

    row_i, col_i = iota((rows, rows), 0), iota((rows, rows), 1)
    eye = row_i == col_i
    lower, strict = row_i >= col_i, row_i > col_i
    same_block = (row_i < BLOCK) == (col_i < BLOCK)

    def to_col(row):
        return jnp.sum(jnp.where(eye, row, 0.0), axis=1, keepdims=True)

    def to_row(col):
        return jnp.sum(jnp.where(eye, col, 0.0), axis=0, keepdims=True)

    queries = vm["probe"][...].astype(F32)
    keys = vm["address"][...].astype(F32)
    values = vm["content"][...].astype(F32)
    q_unit = queries * lax.rsqrt(
        jnp.sum(queries * queries, -1, keepdims=True) + 1e-06
    ) * queries.shape[-1] ** (-0.5)
    k_unit = keys * lax.rsqrt(jnp.sum(keys * keys, -1, keepdims=True) + 1e-06)
    gate = to_col(1.0 / (1.0 + jnp.exp(-vm["storage"][...])))
    fade = vm["fade"][...]
    softplus = jnp.maximum(fade, 0.0) + jnp.log(1.0 + jnp.exp(-jnp.abs(fade)))
    rate = jnp.exp(vm["channel"][...])
    decay = vm["extra"][...] - rate * softplus
    c_col = jnp.sum(jnp.where(lower, decay, 0.0), axis=1, keepdims=True)
    c_row = to_row(c_col)
    label_row = vm["label"][...].astype(F32)
    label_col = to_col(label_row)
    label_first, label_last = label_row[:, :1], label_row[:, rows - 1 :]
    c_last = c_row[:, rows - 1 :]
    reach = jnp.where(
        lower & (label_col == label_row), jnp.exp(jnp.where(lower, c_col - c_row, 0.0)), 0.0
    )
    weighted = k_unit * gate
    coupling = jnp.where(strict, mm_nt(weighted, k_unit) * reach, 0.0)
    power = jnp.where(same_block, coupling, 0.0)
    across = jnp.where(same_block, 0.0, coupling)
    inverse = jnp.where(eye, 1.0, 0.0) - power
    for _ in range(BLOCK.bit_length() - 2):
        power = mm(power, power)
        inverse = inverse + mm(inverse, power)
    inverse = inverse - mm(inverse, mm(across, inverse))
    growth = jnp.exp(c_col) * (label_col == label_first).astype(F32)
    both = mm(inverse, jnp.concatenate([weighted * growth, values * gate], axis=1))
    tail_keys = k_unit * (jnp.exp(c_last - c_col) * (label_col == label_last).astype(F32))
    ends = mm_tn(tail_keys, both)
    end_growth = jnp.exp(c_last) * (label_last == label_first).astype(F32)
    scores = mm_nt(q_unit, k_unit) * reach
    outs = mm(scores, both)
    width = q_unit.shape[-1]
    q_grown = q_unit * growth - outs[:, :width]
    own_mixed = outs[:, width:]
    state_map = (jnp.where(eye, end_growth, 0.0) - ends[:, :width]).astype(BF16)
    shift = ends[:, width:]
    marks_at = width + 16
    pay[0:width, :] = shift.astype(BF16)
    pay[width : width + 8, :] = jnp.broadcast_to(label_first, (8, width)).astype(BF16)
    pay[width + 8 : marks_at, :] = jnp.broadcast_to(label_last, (8, width)).astype(BF16)
    pay[marks_at:, :] = state_map
    pl.semaphore_wait(barrier, n_sp + n_tp - 2)
    tops = [pay.shape[0]] * (REACH - 1) + [marks_at]
    first = [
        remote(
            pay.at[0:top], pieces.at[k, 0:top], pa_s.at[k], pa_r.at[k],
            at_sp(lax.rem(s + k + 1, n_sp)),
        )
        for k, top in enumerate(tops)
    ]
    for k in reversed(range(REACH)):
        first[k].start()

    for name in names:
        if name not in early:
            loads[name].wait()
    pick0, pick1 = vm["picks"][0:1, :], vm["picks"][1:2, :]
    share = vm["share"][...].astype(F32)
    expert_i = iota((experts, rows), 0)
    to0, to1 = (expert_i == pick0).astype(F32), (expert_i == pick1).astype(F32)
    chosen = to0 + to1
    rank = mm(chosen, (row_i < col_i).astype(F32))
    coded = jnp.where(chosen > 0.0, rank + 1.0, 0.0)
    shares = to0 * share[0:1, :] + to1 * share[1:2, :]
    slot_i = iota((padded, experts), 0)
    from_e = iota((padded, experts), 1) * stride
    spread = ((slot_i >= from_e) & (slot_i < from_e + stride)).astype(F32)
    place = iota((n_sp, stride, rows), 1).reshape(padded, rows)
    wide = mm(spread, jnp.concatenate([coded, shares, to0], axis=1))
    hot = wide[:, :rows] == (place + 1).astype(F32)
    dispatch = hot.astype(BF16)
    slot_share = jnp.sum(jnp.where(hot, wide[:, rows : 2 * rows], 0.0), axis=1, keepdims=True)
    slot_first = jnp.sum(jnp.where(hot, wide[:, 2 * rows :], 0.0), axis=1, keepdims=True)
    here = (iota((padded, rows), 1) == place).astype(F32)

    def per_slot(column):
        return jnp.sum((here * column).reshape(n_sp, stride, rows), axis=1, keepdims=True)

    told[...] = jnp.zeros_like(told)
    told[:, 0:1, :] = per_slot(slot_share).astype(BF16)
    told[:, 1:2, :] = per_slot(slot_first).astype(BF16)
    compact_i = iota((slots, padded), 0).astype(F32)
    source = jnp.floor((compact_i + 0.5) * (1.0 / cap))
    within = compact_i - source * cap
    column = iota((slots, padded), 1).astype(F32)
    compact = (column == source * stride + within).astype(BF16)
    slot_lane = iota((slots, rows), 1).astype(F32) == within[:, :rows]
    valve = silu(vm["exit"][...].astype(F32))

    for k in range(REACH):
        first[k].wait_recv()

    def piece(k):
        label = pieces[k, width:marks_at, :].astype(F32)
        return pieces[k, 0:width, :], label[0:1, :], label[8:9, :]

    shift1, first1, last1 = piece(0)
    shift2, first2, last2 = piece(1)
    shift3, _, last3 = piece(2)
    map1 = pieces[0, marks_at:, :] * (first1 == last2).astype(BF16)
    map2 = pieces[1, marks_at:, :] * (first2 == last3).astype(BF16)
    joined = (label_first == last1).astype(F32)
    shift12 = shift1.astype(F32) + mm(map1, shift2)
    map12 = mm(map1, map2).astype(BF16)
    entering = (shift12 + mm(map12, shift3)) * joined
    carry_out[...] = (shift + mm(state_map, entering)).astype(BF16)
    second = remote(
        carry_out, carry_in, pb_s.at[0], pb_s.at[1], at_sp(lax.rem(s + REACH, n_sp))
    )
    second.start()
    second.wait_recv()
    incoming = (shift12 + mm(map12, carry_in[...])) * joined
    mixed = own_mixed + mm(q_grown, incoming)
    scaled = mixed * lax.rsqrt(jnp.mean(mixed * mixed, -1, keepdims=True) + 1e-06)
    heads_out = (scaled * valve).astype(BF16)

    far_first = sorted(range(1, ny), key=lambda k: -min(k, ny - k))

    def scattered_sum(part, pair, send, recv, d_r, y_r):
        near = {}
        for k in far_first + [0]:
            chip = lax.rem(y + k, ny)
            near[k] = remote(
                part.at[chip, other], pair.at[chip], d_r.at[ny], d_r.at[k], at_tp(2 * y + other)
            )
            near[k].start()
        for k in far_first:
            chip = lax.rem(y + k, ny)
            near[k].wait_recv()
            send[chip] = (part[chip, c].astype(F32) + pair[chip].astype(F32)).astype(BF16)
            remote(send.at[chip], recv.at[k], y_r.at[1], y_r.at[0], at_tp(2 * chip + c)).start()
        near[0].wait_recv()
        total = part[y, c].astype(F32) + pair[y].astype(F32)
        if far_first:
            there = recv.at[1:ny]
            remote(there, there, y_r.at[1], y_r.at[0], at_tp(t)).wait_recv()
            for k in far_first:
                total = total + recv[k].astype(F32)
        return total

    def sums_left(part, recv, d_r, y_r):
        remote(part.at[:, 0], part.at[:, 0], d_r.at[ny], d_r.at[ny], at_tp(t)).wait_send()
        if far_first:
            there = recv.at[1:ny]
            remote(there, there, y_r.at[1], y_r.at[0], at_tp(t)).wait_send()

    def tell(stat, sems, line):
        stat[t] = line
        for k in range(1, n_tp):
            to = lax.rem(t + k, n_tp)
            remote(stat.at[t], stat.at[t], sems.at[0], sems.at[1], at_tp(to)).start()

    def heard_all(stat, sems):
        there = stat.at[1:n_tp]
        remote(there, there, sems.at[0], sems.at[1], at_tp(t)).wait()
        return jnp.sum(stat[...], axis=0)

    scaled_in = ALPHA * vm["incoming"][...].astype(F32)
    row_sum = jnp.sum(scaled_in, -1, keepdims=True)
    for chip in range(ny):
        product = mm(heads_out, vm["final"][:, chip * 2 * width : (chip + 1) * 2 * width])
        part1[chip, 0] = product[:, :width].astype(BF16)
        part1[chip, 1] = product[:, width:].astype(BF16)
        row_sum = row_sum + jnp.sum(product, -1, keepdims=True)
    tell(stat0, mean_s, to_row(row_sum))
    projected = scattered_sum(part1, pair1, send1, recv1, d1_r, y1_r)
    features = width * n_tp
    mean = to_col(heard_all(stat0, mean_s) / features)
    centred = scaled_in + projected - mean

    nx = 4
    nz = n_sp // nx
    hops = sorted(
        ((dz, dx) for dz in range(nz) for dx in range(nx) if dz or dx),
        key=lambda d: -min(d[0], nz - d[0]) - min(d[1], nx - d[1]),
    )

    def scatter(src, dst, sems):
        z, x = s // nx, lax.rem(s, nx)
        for dz, dx in hops:
            to = lax.rem(z + dz, nz) * nx + lax.rem(x + dx, nx)
            remote(src.at[to], dst.at[s], sems.at[0], sems.at[1], at_sp(to)).start()
        dst[s] = src[s]

    def collected(dst, sems):
        there = dst.at[1:n_sp]
        remote(there, there, sems.at[0], sems.at[1], at_sp(s)).wait()
        return dst[...].reshape(dst.shape[0] * dst.shape[1], dst.shape[2])

    gained = (centred * vm["gain1"][...]).astype(BF16)
    payload = jnp.dot(dispatch, gained, preferred_element_type=F32)
    sent[...] = payload.astype(BF16).reshape(n_sp, stride, rows)
    scatter(sent, arrived, dis_s)
    tell(stat1, sq1_s, to_row(jnp.sum(centred * centred, -1, keepdims=True)))
    row_scale = lax.rsqrt(heard_all(stat1, sq1_s) / features + 1e-05)
    slot_scale = jnp.sum(jnp.where(hot, row_scale, 0.0), axis=1, keepdims=True)
    scales = per_slot(slot_scale)
    coarse = scales.astype(BF16)
    told[:, 2:3, :] = coarse
    told[:, 3:4, :] = (scales - coarse.astype(F32)).astype(BF16)
    scatter(told, heard, note_s)
    middle = (centred * to_col(row_scale) * vm["gain1"][...]).astype(BF16)
    came = collected(arrived, dis_s)
    own_rows = jnp.dot(compact, came, preferred_element_type=F32).astype(BF16)

    lanes = pl.ds(pl.multiple_of(c * width, width), width)
    ahead = lax.rem(y + 1 - 2 * c + ny, ny)
    behind = lax.rem(y - 1 + 2 * c + ny, ny)
    most, least = ny // 2, (ny - 1) // 2

    def origin(k):
        return lax.rem(y - k * (1 - 2 * c) + 2 * ny, ny)

    gathered[y, :, lanes] = own_rows

    def block(chip):
        return gathered.at[chip, :, lanes]

    def hand(k, chip):
        return remote(block(chip), block(chip), gone_s.at[0], own_r.at[k], at_tp(2 * y + other))

    def big(k):
        chip = origin(k)
        return remote(block(chip), block(chip), gone_s.at[1], big_r.at[k], at_tp(2 * ahead + c))

    def small(k):
        chip = origin(-k)
        return remote(
            block(chip), block(chip), gone_s.at[1], small_r.at[k], at_tp(2 * behind + c)
        )

    def big_wait(k):
        chip = origin(k + 1)
        remote(
            block(chip), block(chip), gone_s.at[1], big_r.at[k], at_tp(2 * ahead + c)
        ).wait_recv()

    def small_wait(k):
        chip = origin(-k - 1)
        remote(
            block(chip), block(chip), gone_s.at[1], small_r.at[k], at_tp(2 * behind + c)
        ).wait_recv()

    def hand_wait(k, chip):
        other_lanes = pl.ds(pl.multiple_of(other * width, width), width)
        there = gathered.at[chip, :, other_lanes]
        remote(there, there, gone_s.at[0], own_r.at[k], at_tp(2 * y + other)).wait_recv()

    def absorb(chip, fresh):
        block_in = gathered[chip]
        at = pl.ds(pl.multiple_of(chip * 2 * width, 2 * width), 2 * width)
        gates = jnp.dot(block_in, vm["valve"][at, :], preferred_element_type=F32)
        ups = jnp.dot(block_in, vm["raise"][at, :], preferred_element_type=F32)
        common = lax.dot_general(
            block_in, vm["common"][:, at], (((1,), (1,)), ((), ())), preferred_element_type=F32
        )
        if fresh:
            acc_g[0], acc_g[1], acc_s[...] = gates, ups, common
        else:
            acc_g[0] += gates
            acc_g[1] += ups
            acc_s[...] += common

    big(0).start()
    if least:
        small(0).start()
    hand(0, y).start()
    hand_wait(0, y)
    absorb(y, True)
    for k in range(1, most + 1):
        big_wait(k - 1)
        if k < most:
            big(k).start()
        hand(2 * k - 1, origin(k)).start()
        if k <= least:
            small_wait(k - 1)
            if k < least:
                small(k).start()
            hand(2 * k, origin(-k)).start()
        hand_wait(2 * k - 1, origin(-k))
        absorb(origin(-k), False)
        if k <= least:
            hand_wait(2 * k, origin(k))
            absorb(origin(k), False)

    notes = collected(heard, note_s)

    note_column = iota((slots, notes.shape[0]), 1).astype(F32)
    note_source = source[:, :1] * told.shape[1]

    def noted(j):
        line = (note_column == note_source + j).astype(BF16)
        found = jnp.dot(line, notes, preferred_element_type=F32)
        return jnp.sum(jnp.where(slot_lane, found, 0.0), axis=1, keepdims=True)

    weight, flag, scale = noted(0), noted(1), noted(2) + noted(3)
    hidden = (silu(acc_g[0] * scale) * acc_g[1] * (scale * weight)).astype(BF16)
    common = acc_s[...] * scale
    shared = (silu(common[:, :sf]) * common[:, sf:] * flag).astype(BF16)
    for chip in range(ny):
        at = slice(chip * 2 * width, (chip + 1) * 2 * width)
        product = jnp.dot(hidden, vm["lower"][:, at], preferred_element_type=F32) + jnp.dot(
            shared, vm["common_low"][:, at], preferred_element_type=F32
        )
        part2[chip, 0] = product[:, :width].astype(BF16)
        part2[chip, 1] = product[:, width:].astype(BF16)
    summed = scattered_sum(part2, pair2, send2, recv2, d2_r, y2_r)

    rsend[...] = mm_tn(compact, summed).astype(BF16).reshape(n_sp, stride, rows)
    scatter(rsend, returned, ret_s)
    back = collected(returned, ret_s)
    mixture = mm_tn(dispatch, back)
    second_sum = ALPHA * middle.astype(F32) + mixture
    sums = [jnp.sum(v, -1, keepdims=True) for v in (second_sum, second_sum * second_sum)]
    tell(stat2, sq2_s, jnp.concatenate([to_row(v) for v in sums], axis=0))
    totals = heard_all(stat2, sq2_s) / features
    mean2, square2 = totals[0:1, :], totals[1:2, :]
    scale2 = lax.rsqrt(square2 - mean2 * mean2 + 1e-05)
    out_vm[...] = (
        (second_sum - to_col(mean2)) * to_col(scale2) * vm["gain2"][...]
    ).astype(BF16)
    out_copy = pltpu.make_async_copy(out_vm, out_hbm, out_sem)
    out_copy.start()

    for copy in first:
        copy.wait_send()
    second.wait_send()
    remote(send2, send2, gone_s.at[0], gone_s.at[0], at_tp(t)).wait_send()
    if far_first:
        there = send2.at[1:ny]
        remote(there, there, gone_s.at[1], gone_s.at[1], at_tp(t)).wait_send()
    sums_left(part1, recv1, d1_r, y1_r)
    sums_left(part2, recv2, d2_r, y2_r)
    out_copy.wait()


def dims_names():
    return (
        "probe", "address", "content", "storage", "fade", "extra", "label",
        "picks", "share", "exit", "incoming", "gain1", "gain2", "final",
        "valve", "raise", "lower", "common", "common_raise", "common_low", "channel",
    )


def shards(
    probe, address, content, storage, fade, channel, extra, label, exit_valve, final,
    incoming, gain1, picks, share, valve, raising, lowering, common_valve, common_raising,
    common_lowering, gain2,
):
    n_sp, n_tp = lax.axis_size("sp"), lax.axis_size("tp")
    ny = n_tp // 2
    rows, width = probe.shape
    experts = n_sp * valve.shape[0]
    cap = max(2, 9 * rows * picks.shape[1] // (8 * experts))
    stride = -(-(cap + 2) // 16) * 16
    slots = n_sp * cap
    ff, features = valve.shape[2], valve.shape[1]
    sf = common_valve.shape[1]
    dims = (n_sp, n_tp, rows, experts, cap, stride)
    args = {
        "probe": probe, "address": address, "content": content, "storage": storage,
        "fade": fade, "extra": extra, "label": label[None, :], "picks": picks.T,
        "share": share.T, "exit": exit_valve, "incoming": incoming, "gain1": gain1[None, :],
        "gain2": gain2[None, :], "final": final, "valve": valve[0], "raise": raising[0],
        "lower": lowering[0],
        "common": common_valve.T, "common_raise": common_raising.T,
        "common_low": common_lowering, "channel": channel[None, :],
    }
    names = dims_names()
    operands = [args[n] for n in names]
    dma = pltpu.SemaphoreType.DMA
    shapes = {n: a.shape for n, a in args.items()}
    shapes["common"] = (2 * sf, features)
    shapes["common_raise"] = (8, 128)
    own = [pltpu.VMEM(shapes[n], args[n].dtype) for n in names]

    def vmem(*shape, kind=BF16):
        return pltpu.VMEM(shape, kind)

    return pl.pallas_call(
        functools.partial(kernel, dims),
        out_shape=jax.ShapeDtypeStruct((rows, width), BF16),
        in_specs=[pl.BlockSpec(memory_space=pl.ANY)] * len(operands),
        out_specs=pl.BlockSpec(memory_space=pl.ANY),
        scratch_shapes=own
        + [
            vmem(2 * width + 16, width), vmem(REACH, 2 * width + 16, width),
            vmem(width, width), vmem(width, width),
            vmem(ny, 2, rows, width), vmem(ny, rows, width), vmem(ny, rows, width),
            vmem(ny, rows, width),
            vmem(n_tp, 1, rows, kind=F32), vmem(n_tp, 1, rows, kind=F32),
            vmem(n_tp, 2, rows, kind=F32),
            vmem(n_sp, stride, width), vmem(n_sp, stride, width),
            vmem(n_sp, 16, width), vmem(n_sp, 16, width),
            vmem(ny, slots, 2 * width), vmem(2, slots, ff, kind=F32), vmem(slots, 2 * sf, kind=F32),
            vmem(ny, 2, slots, width), vmem(ny, slots, width), vmem(ny, slots, width),
            vmem(ny, slots, width),
            vmem(n_sp, stride, width), vmem(n_sp, stride, width), vmem(rows, width),
            dma((len(operands),)), dma, dma((REACH,)), dma((REACH,)), dma((2,)),
            dma((ny + 1,)), dma((2,)), dma((2,)), dma((2,)), dma((2,)),
            dma((2,)), dma((2,)), dma((2,)), dma((ny,)), dma((ny,)), dma((ny,)), dma((2,)),
            dma((ny + 1,)), dma((2,)),
        ],
        compiler_params=pltpu.CompilerParams(
            collective_id=0, has_side_effects=True, vmem_limit_bytes=60 * 1024 * 1024
        ),
        name="layer",
    )(*operands)


def solution(mesh):
    return jax.shard_map(
        shards,
        mesh=mesh,
        in_specs=(
            P("sp", "tp"), P("sp", "tp"), P("sp", "tp"), P("tp", "sp"), P("tp", "sp"), P("tp"),
            P("tp", "sp"), P("sp"), P("sp", "tp"), P("tp", None), P("sp", "tp"), P("tp"),
            P("sp", None), P("sp", None), P("sp", None, "tp"), P("sp", None, "tp"),
            P("sp", "tp", None), P(None, "tp"), P(None, "tp"), P("tp", None), P("tp"),
        ),
        out_specs=P("sp", "tp"),
        check_vma=False,
    )
```

time: 104 us -> 92.2 us (0.89)
  Pallas kernels: 99.6 us -> 90 us
  other arithmetic: 1.68 us -> 0 us
    pallas_call x1, Pallas kernels: 99.6 us -> 90 us  [shards(): pl.pallas_call(functools.partial(kernel, dims), out_shape=jax.ShapeDtypeS...]
    concatenate x1 -> x0, other arithmetic: 1.68 us -> none  [shards(): jnp.concatenate([common_valve.T, common_raising.T], axis=0)]
where the time goes in v2:
time: 92.2 us; the launch traced here: 92 us
  Pallas kernels  90 us (98%)
  local copies, waits for them, and re-layouts  1.38 us (1%)
    pallas_call x1, Pallas kernels, shards(): pl.pallas_call(functools.partial(kernel, dims), out_shape=jax.ShapeDtypeS...  90 us

profile of v2, /device:TPU:1, one launch (start us, length us, event | category | flops | bytes accessed | tf_op | source)
XLA Modules:
  0.0 92.0 jit_solution(11938211126500096516)
XLA Ops:
  0.7 90.0 %layer.1 = bf16[128,128]{1,0:T(8,128)(2,1)} custom-call(bf16[128,128]{1,0:T(8,128)(2,1)} %refs_0_.1, bf16[128,128]{1,0:T(8,128)(2,1)} %refs_1_.1, bf16[128,128]{1,0:T(8,128)(2,1)} %refs_2_.1, f32[1,128]{1,0:T(1,128)} %refs_3_.1, f32[1,128]{1,0:T(1,128)} %refs_4_.1, f32[1,128]{1,0:T(1,128)} %refs_5_.1, s32[1,128]{1,0:T(1,128)} %bitcast.18, ...), custom_call_target="tpu_custom_call" | custom-call | tf_op jit(solution)/shard_map/layer/pallas_call | solution.py:513
  90.7 1.4 %copy.24 = bf16[128,128]{1,0:T(8,128)(2,1)} copy(bf16[128,128]{1,0:T(8,128)(2,1)} %layer.1) | data formatting | bytes 65536

commit v3 on v2

--- a/solution.py
+++ b/solution.py
@@ -13,6 +13,7 @@
 BF16 = jnp.bfloat16
 MESH = pl.DeviceIdType.MESH
 REACH = 3
+CHUNKS = 2
 
 
 def iota(shape, dim):
@@ -54,12 +55,12 @@
         part1, pair1, send1, recv1,
         stat0, stat1, stat2,
         sent, arrived, told, heard, gathered, acc_g, acc_s,
-        part2, pair2, send2, recv2,
+        part2, pair2, send2, recv2, send3, recv3,
         rsend, returned, out_vm,
         load_sem, out_sem, pa_s, pa_r, pb_s,
         d1_r, y1_r, mean_s, sq1_s, sq2_s,
         dis_s, note_s, ret_s, big_r, small_r, own_r, gone_s,
-        d2_r, y2_r,
+        near_r, far_r, back_r,
     ) = scratch[len(names) :]
 
     s = lax.axis_index("sp")
@@ -290,8 +291,10 @@
 
     scaled_in = ALPHA * vm["incoming"][...].astype(F32)
     row_sum = jnp.sum(scaled_in, -1, keepdims=True)
-    for chip in range(ny):
-        product = mm(heads_out, vm["final"][:, chip * 2 * width : (chip + 1) * 2 * width])
+    for k in far_first + [0]:
+        chip = lax.rem(y + k, ny)
+        at = pl.ds(pl.multiple_of(chip * 2 * width, 2 * width), 2 * width)
+        product = mm(heads_out, vm["final"][:, at])
         part1[chip, 0] = product[:, :width].astype(BF16)
         part1[chip, 1] = product[:, width:].astype(BF16)
         row_sum = row_sum + jnp.sum(product, -1, keepdims=True)
@@ -325,6 +328,88 @@
     sent[...] = payload.astype(BF16).reshape(n_sp, stride, rows)
     scatter(sent, arrived, dis_s)
     tell(stat1, sq1_s, to_row(jnp.sum(centred * centred, -1, keepdims=True)))
+    came = collected(arrived, dis_s)
+    own_rows = jnp.dot(compact, came, preferred_element_type=F32).astype(BF16)
+
+    lanes = pl.ds(pl.multiple_of(c * width, width), width)
+    turn = 1 - 2 * c
+    ahead = lax.rem(y + turn + ny, ny)
+    behind = lax.rem(y - turn + ny, ny)
+    most, least = ny // 2, (ny - 1) // 2
+    piece_rows = slots // CHUNKS
+
+    def rows_of(q):
+        return slice(q * piece_rows, (q + 1) * piece_rows)
+
+    def along(d):
+        return lax.rem(y + d * turn + 2 * ny, ny)
+
+    gathered[y, :, lanes] = own_rows
+
+    def block(chip, q):
+        return gathered.at[chip, rows_of(q), lanes]
+
+    def passed(chip, q, sem, to):
+        there = block(chip, q)
+        return remote(there, there, gone_s.at[1], sem, at_tp(2 * to + c))
+
+    def big(k, q, origin):
+        return passed(along(-origin), q, big_r.at[k * CHUNKS + q], ahead)
+
+    def small(k, q, origin):
+        return passed(along(origin), q, small_r.at[k * CHUNKS + q], behind)
+
+    def chips_at(k):
+        return [along(k)] if k == 0 or k > least else [along(-k), along(k)]
+
+    def hand(k, q):
+        for chip in reversed(chips_at(k)):
+            there = block(chip, q)
+            remote(
+                there, there, gone_s.at[0], own_r.at[k * CHUNKS + q], at_tp(2 * y + other)
+            ).start()
+
+    def wait_bytes(count, sem):
+        there = pair2.at[0:count, 0:piece_rows]
+        remote(there, there, sem, sem, at_tp(t)).wait_recv()
+
+    def absorb(k, q):
+        chips, at_rows = chips_at(k), rows_of(q)
+        wait_bytes(len(chips), own_r.at[k * CHUNKS + q])
+        for chip in chips:
+            block_in = gathered[chip, at_rows, :]
+            at = pl.ds(pl.multiple_of(chip * 2 * width, 2 * width), 2 * width)
+            gates = jnp.dot(block_in, vm["valve"][at, :], preferred_element_type=F32)
+            ups = jnp.dot(block_in, vm["raise"][at, :], preferred_element_type=F32)
+            common = lax.dot_general(
+                block_in, vm["common"][:, at], (((1,), (1,)), ((), ())), preferred_element_type=F32
+            )
+            if k == 0:
+                acc_g[0, at_rows], acc_g[1, at_rows], acc_s[at_rows] = gates, ups, common
+            else:
+                acc_g[0, at_rows] += gates
+                acc_g[1, at_rows] += ups
+                acc_s[at_rows] += common
+
+    def all_noted():
+        notes = collected(heard, note_s)
+        note_column = iota((slots, notes.shape[0]), 1).astype(F32)
+        note_source = source[:, :1] * told.shape[1]
+
+        def noted(j):
+            line = (note_column == note_source + j).astype(BF16)
+            found = jnp.dot(line, notes, preferred_element_type=F32)
+            return jnp.sum(jnp.where(slot_lane, found, 0.0), axis=1, keepdims=True)
+
+        return noted(0), noted(1), noted(2) + noted(3)
+
+    for q in range(CHUNKS):
+        if most:
+            big(0, q, 0).start()
+        if least:
+            small(0, q, 0).start()
+    for q in range(CHUNKS):
+        hand(0, q)
     row_scale = lax.rsqrt(heard_all(stat1, sq1_s) / features + 1e-05)
     slot_scale = jnp.sum(jnp.where(hot, row_scale, 0.0), axis=1, keepdims=True)
     scales = per_slot(slot_scale)
@@ -333,114 +418,111 @@
     told[:, 3:4, :] = (scales - coarse.astype(F32)).astype(BF16)
     scatter(told, heard, note_s)
     middle = (centred * to_col(row_scale) * vm["gain1"][...]).astype(BF16)
-    came = collected(arrived, dis_s)
-    own_rows = jnp.dot(compact, came, preferred_element_type=F32).astype(BF16)
-
-    lanes = pl.ds(pl.multiple_of(c * width, width), width)
-    ahead = lax.rem(y + 1 - 2 * c + ny, ny)
-    behind = lax.rem(y - 1 + 2 * c + ny, ny)
-    most, least = ny // 2, (ny - 1) // 2
-
-    def origin(k):
-        return lax.rem(y - k * (1 - 2 * c) + 2 * ny, ny)
-
-    gathered[y, :, lanes] = own_rows
-
-    def block(chip):
-        return gathered.at[chip, :, lanes]
-
-    def hand(k, chip):
-        return remote(block(chip), block(chip), gone_s.at[0], own_r.at[k], at_tp(2 * y + other))
-
-    def big(k):
-        chip = origin(k)
-        return remote(block(chip), block(chip), gone_s.at[1], big_r.at[k], at_tp(2 * ahead + c))
-
-    def small(k):
-        chip = origin(-k)
+    waiting = [(0, q) for q in range(CHUNKS)]
+    slot_notes = None
+    for k in range(1, most + 1):
+        for q in range(CHUNKS):
+            big(k - 1, q, k).wait_recv()
+            if k < most:
+                big(k, q, k).start()
+            if k <= least:
+                small(k - 1, q, k).wait_recv()
+                if k < least:
+                    small(k, q, k).start()
+            hand(k, q)
+            absorb(*waiting.pop(0))
+            waiting.append((k, q))
+        if k == most - 1:
+            slot_notes = all_noted()
+    if slot_notes is None:
+        slot_notes = all_noted()
+
+    def expert(q):
+        at_rows = rows_of(q)
+        weight, flag, scale = (v[at_rows] for v in slot_notes)
+        hidden = (silu(acc_g[0, at_rows] * scale) * acc_g[1, at_rows] * (scale * weight)).astype(
+            BF16
+        )
+        common = acc_s[at_rows] * scale
+        shared = (silu(common[:, :sf]) * common[:, sf:] * flag).astype(BF16)
+        for chip in range(ny):
+            at = slice(chip * 2 * width, (chip + 1) * 2 * width)
+            product = jnp.dot(hidden, vm["lower"][:, at], preferred_element_type=F32) + jnp.dot(
+                shared, vm["common_low"][:, at], preferred_element_type=F32
+            )
+            part2[chip, 0, at_rows] = product[:, :width].astype(BF16)
+            part2[chip, 1, at_rows] = product[:, width:].astype(BF16)
+        for g, group in enumerate(groups):
+            for d in group:
+                chip = along(d)
+                remote(
+                    part2.at[chip, other, at_rows], pair2.at[chip, at_rows], gone_s.at[2],
+                    near_r.at[2 * q + g], at_tp(2 * y + other),
+                ).start()
+
+    soon = sorted({most % ny, least % ny, -least % ny} - {0})
+    groups = [soon, [d for d in range(ny) if d not in soon]]
+    for q in range(CHUNKS):
+        absorb(*waiting.pop(0))
+        expert(q)
+
+    def chip_sum(d, q):
+        chip, at_rows = along(d), rows_of(q)
+        return part2[chip, c, at_rows].astype(F32) + pair2[chip, at_rows].astype(F32)
+
+    def ring_step(j, q, reach, sign, send, recv, sem, gone, to):
+        at_rows = rows_of(q)
+        value = chip_sum(sign * (reach - j), q)
+        if j:
+            came_in(j - 1, q, send, recv, sem, gone, to).wait_recv()
+            value = value + recv[j - 1, at_rows].astype(F32)
+        send[j, at_rows] = value.astype(BF16)
+        came_in(j, q, send, recv, sem, gone, to).start()
+
+    def came_in(j, q, send, recv, sem, gone, to):
+        at_rows = rows_of(q)
         return remote(
-            block(chip), block(chip), gone_s.at[1], small_r.at[k], at_tp(2 * behind + c)
+            send.at[j, at_rows], recv.at[j, at_rows], gone, sem.at[j * CHUNKS + q],
+            at_tp(2 * to + c),
         )
 
-    def big_wait(k):
-        chip = origin(k + 1)
-        remote(
-            block(chip), block(chip), gone_s.at[1], big_r.at[k], at_tp(2 * ahead + c)
-        ).wait_recv()
-
-    def small_wait(k):
-        chip = origin(-k - 1)
-        remote(
-            block(chip), block(chip), gone_s.at[1], small_r.at[k], at_tp(2 * behind + c)
-        ).wait_recv()
-
-    def hand_wait(k, chip):
-        other_lanes = pl.ds(pl.multiple_of(other * width, width), width)
-        there = gathered.at[chip, :, other_lanes]
-        remote(there, there, gone_s.at[0], own_r.at[k], at_tp(2 * y + other)).wait_recv()
-
-    def absorb(chip, fresh):
-        block_in = gathered[chip]
-        at = pl.ds(pl.multiple_of(chip * 2 * width, 2 * width), 2 * width)
-        gates = jnp.dot(block_in, vm["valve"][at, :], preferred_element_type=F32)
-        ups = jnp.dot(block_in, vm["raise"][at, :], preferred_element_type=F32)
-        common = lax.dot_general(
-            block_in, vm["common"][:, at], (((1,), (1,)), ((), ())), preferred_element_type=F32
+    large = (send2, recv2, far_r, gone_s.at[3], ahead)
+    little = (send3, recv3, back_r, gone_s.at[4], behind)
+    for j in range(most):
+        for q in range(CHUNKS):
+            if j < 2 and groups[j]:
+                wait_bytes(len(groups[j]), near_r.at[2 * q + j])
+            ring_step(j, q, most, 1, *large)
+            if j < least:
+                ring_step(j, q, least, -1, *little)
+    for q in range(CHUNKS):
+        if most < 2:
+            wait_bytes(len(groups[1]), near_r.at[2 * q + 1])
+        value = chip_sum(0, q)
+        if most:
+            came_in(most - 1, q, *large).wait_recv()
+            value = value + recv2[most - 1, rows_of(q)].astype(F32)
+        if least:
+            came_in(least - 1, q, *little).wait_recv()
+            value = value + recv3[least - 1, rows_of(q)].astype(F32)
+        share_sp = n_sp // CHUNKS
+        owners = slice(q * share_sp, (q + 1) * share_sp)
+        spots = slice(q * share_sp * stride, (q + 1) * share_sp * stride)
+        rsend[owners] = (
+            mm_tn(compact[rows_of(q), spots], value)
+            .astype(BF16)
+            .reshape(share_sp, stride, rows)
         )
-        if fresh:
-            acc_g[0], acc_g[1], acc_s[...] = gates, ups, common
-        else:
-            acc_g[0] += gates
-            acc_g[1] += ups
-            acc_s[...] += common
-
-    big(0).start()
-    if least:
-        small(0).start()
-    hand(0, y).start()
-    hand_wait(0, y)
-    absorb(y, True)
-    for k in range(1, most + 1):
-        big_wait(k - 1)
-        if k < most:
-            big(k).start()
-        hand(2 * k - 1, origin(k)).start()
-        if k <= least:
-            small_wait(k - 1)
-            if k < least:
-                small(k).start()
-            hand(2 * k, origin(-k)).start()
-        hand_wait(2 * k - 1, origin(-k))
-        absorb(origin(-k), False)
-        if k <= least:
-            hand_wait(2 * k, origin(k))
-            absorb(origin(k), False)
-
-    notes = collected(heard, note_s)
-
-    note_column = iota((slots, notes.shape[0]), 1).astype(F32)
-    note_source = source[:, :1] * told.shape[1]
-
-    def noted(j):
-        line = (note_column == note_source + j).astype(BF16)
-        found = jnp.dot(line, notes, preferred_element_type=F32)
-        return jnp.sum(jnp.where(slot_lane, found, 0.0), axis=1, keepdims=True)
-
-    weight, flag, scale = noted(0), noted(1), noted(2) + noted(3)
-    hidden = (silu(acc_g[0] * scale) * acc_g[1] * (scale * weight)).astype(BF16)
-    common = acc_s[...] * scale
-    shared = (silu(common[:, :sf]) * common[:, sf:] * flag).astype(BF16)
-    for chip in range(ny):
-        at = slice(chip * 2 * width, (chip + 1) * 2 * width)
-        product = jnp.dot(hidden, vm["lower"][:, at], preferred_element_type=F32) + jnp.dot(
-            shared, vm["common_low"][:, at], preferred_element_type=F32
-        )
-        part2[chip, 0] = product[:, :width].astype(BF16)
-        part2[chip, 1] = product[:, width:].astype(BF16)
-    summed = scattered_sum(part2, pair2, send2, recv2, d2_r, y2_r)
-
-    rsend[...] = mm_tn(compact, summed).astype(BF16).reshape(n_sp, stride, rows)
-    scatter(rsend, returned, ret_s)
+        for k in range(share_sp):
+            to = q * share_sp + lax.rem(s + k, share_sp)
+
+            @pl.when(to != s)
+            def _(to=to):
+                remote(
+                    rsend.at[to], returned.at[s], ret_s.at[0], ret_s.at[1], at_sp(to)
+                ).start()
+
+    returned[s] = rsend[s]
     back = collected(returned, ret_s)
     mixture = mm_tn(dispatch, back)
     second_sum = ALPHA * middle.astype(F32) + mixture
@@ -458,12 +540,17 @@
     for copy in first:
         copy.wait_send()
     second.wait_send()
-    remote(send2, send2, gone_s.at[0], gone_s.at[0], at_tp(t)).wait_send()
-    if far_first:
-        there = send2.at[1:ny]
-        remote(there, there, gone_s.at[1], gone_s.at[1], at_tp(t)).wait_send()
+    def all_gone(there, sem):
+        remote(there, there, sem, sem, at_tp(t)).wait_send()
+
+    all_gone(pair2, gone_s.at[0])
+    all_gone(pair2, gone_s.at[2])
+    if most:
+        all_gone(pair2.at[1:ny], gone_s.at[1])
+        all_gone(send2, gone_s.at[3])
+    if least:
+        all_gone(send3, gone_s.at[4])
     sums_left(part1, recv1, d1_r, y1_r)
-    sums_left(part2, recv2, d2_r, y2_r)
     out_copy.wait()
 
 
@@ -489,6 +576,7 @@
     slots = n_sp * cap
     ff, features = valve.shape[2], valve.shape[1]
     sf = common_valve.shape[1]
+    most, least = max(1, ny // 2), max(1, (ny - 1) // 2)
     dims = (n_sp, n_tp, rows, experts, cap, stride)
     args = {
         "probe": probe, "address": address, "content": content, "storage": storage,
@@ -526,13 +614,13 @@
             vmem(n_sp, stride, width), vmem(n_sp, stride, width),
             vmem(n_sp, 16, width), vmem(n_sp, 16, width),
             vmem(ny, slots, 2 * width), vmem(2, slots, ff, kind=F32), vmem(slots, 2 * sf, kind=F32),
-            vmem(ny, 2, slots, width), vmem(ny, slots, width), vmem(ny, slots, width),
-            vmem(ny, slots, width),
+            vmem(ny, 2, slots, width), vmem(ny, slots, width), vmem(most, slots, width),
+            vmem(most, slots, width), vmem(least, slots, width), vmem(least, slots, width),
             vmem(n_sp, stride, width), vmem(n_sp, stride, width), vmem(rows, width),
             dma((len(operands),)), dma, dma((REACH,)), dma((REACH,)), dma((2,)),
             dma((ny + 1,)), dma((2,)), dma((2,)), dma((2,)), dma((2,)),
-            dma((2,)), dma((2,)), dma((2,)), dma((ny,)), dma((ny,)), dma((ny,)), dma((2,)),
-            dma((ny + 1,)), dma((2,)),
+            dma((2,)), dma((2,)), dma((2,)), dma((most * CHUNKS,)), dma((least * CHUNKS,)), dma(((most + 1) * CHUNKS,)), dma((5,)),
+            dma((2 * CHUNKS,)), dma((most * CHUNKS,)), dma((least * CHUNKS,)),
         ],
         compiler_params=pltpu.CompilerParams(
             collective_id=0, has_side_effects=True, vmem_limit_bytes=60 * 1024 * 1024

time: 92.2 us -> 88.5 us (0.960)
  Pallas kernels: 90 us -> 86.3 us
    pallas_call x1, Pallas kernels: 90 us -> 86.3 us  [shards(): pl.pallas_call(functools.partial(kernel, dims), out_shape=jax.ShapeDtypeS...]
where the time goes in v3:
time: 88.5 us; the launch traced here: 88.3 us
  Pallas kernels  86.3 us (98%)
  local copies, waits for them, and re-layouts  1.38 us (2%)
    pallas_call x1, Pallas kernels, shards(): pl.pallas_call(functools.partial(kernel, dims), out_shape=jax.ShapeDtypeS...  86.3 us

profile of v3, /device:TPU:1, one launch (start us, length us, event | category | flops | bytes accessed | tf_op | source)
XLA Modules:
  0.0 88.3 jit_solution(2870415689227364174)
XLA Ops:
  0.7 86.3 %layer.1 = bf16[128,128]{1,0:T(8,128)(2,1)} custom-call(bf16[128,128]{1,0:T(8,128)(2,1)} %refs_0_.1, bf16[128,128]{1,0:T(8,128)(2,1)} %refs_1_.1, bf16[128,128]{1,0:T(8,128)(2,1)} %refs_2_.1, f32[1,128]{1,0:T(1,128)} %refs_3_.1, f32[1,128]{1,0:T(1,128)} %refs_4_.1, f32[1,128]{1,0:T(1,128)} %refs_5_.1, s32[1,128]{1,0:T(1,128)} %bitcast.18, ...), custom_call_target="tpu_custom_call" | custom-call | tf_op jit(solution)/shard_map/layer/pallas_call | solution.py:601
  86.9 1.4 %copy.24 = bf16[128,128]{1,0:T(8,128)(2,1)} copy(bf16[128,128]{1,0:T(8,128)(2,1)} %layer.1) | data formatting | bytes 65536

commit v4 on v3

--- a/solution.py
+++ b/solution.py
@@ -47,7 +47,7 @@
     padded = n_sp * stride
     names = dims_names()
     hbm = dict(zip(names, refs[: len(names)]))
-    out_hbm = refs[len(names)]
+    out_ref = refs[len(names)]
     scratch = refs[len(names) + 1 :]
     vm = dict(zip(names, scratch[: len(names)]))
     (
@@ -55,12 +55,12 @@
         part1, pair1, send1, recv1,
         stat0, stat1, stat2,
         sent, arrived, told, heard, gathered, acc_g, acc_s,
-        part2, pair2, send2, recv2, send3, recv3,
-        rsend, returned, out_vm,
-        load_sem, out_sem, pa_s, pa_r, pb_s,
-        d1_r, y1_r, mean_s, sq1_s, sq2_s,
-        dis_s, note_s, ret_s, big_r, small_r, own_r, gone_s,
-        near_r, far_r, back_r,
+        part2, pair2, send2, recv2,
+        rsend, returned,
+        load_sem, pa_s, pa_r, pb_s,
+        near1_r, far1_r, gone1_s, mean_s, sq1_s, sq2_s,
+        dis_s, note_s, ret_s, wire_r, own_r, gone_s,
+        near2_r, far2_r, gone2_s,
     ) = scratch[len(names) :]
 
     s = lax.axis_index("sp")
@@ -248,35 +248,89 @@
     scaled = mixed * lax.rsqrt(jnp.mean(mixed * mixed, -1, keepdims=True) + 1e-06)
     heads_out = (scaled * valve).astype(BF16)
 
-    far_first = sorted(range(1, ny), key=lambda k: -min(k, ny - k))
-
-    def scattered_sum(part, pair, send, recv, d_r, y_r):
-        near = {}
-        for k in far_first + [0]:
-            chip = lax.rem(y + k, ny)
-            near[k] = remote(
-                part.at[chip, other], pair.at[chip], d_r.at[ny], d_r.at[k], at_tp(2 * y + other)
+    def along(d):
+        return lax.rem(y + d + 2 * ny, ny)
+
+    def sigma_of(q):
+        return 1 if q % 2 == 0 else -1
+
+    soon, rest = (3, -3, 4), (1, -1, 2, -2, 0)
+
+    class TpSum:
+        def __init__(self, part, pair, send, recv, near_r, far_r, gone, chunk_rows):
+            self.part, self.pair, self.send, self.recv = part, pair, send, recv
+            self.near_r, self.far_r, self.gone, self.rows = near_r, far_r, gone, chunk_rows
+
+        def at(self, q):
+            return slice(q * self.rows, (q + 1) * self.rows)
+
+        def put(self, d, at_rows, product):
+            chip = along(d)
+            self.part[chip, 0, at_rows] = product[:, :width].astype(BF16)
+            self.part[chip, 1, at_rows] = product[:, width:].astype(BF16)
+
+        def near(self, q, g):
+            for d in (soon, rest)[g]:
+                chip = along(d)
+                remote(
+                    self.part.at[chip, other, self.at(q)], self.pair.at[chip, self.at(q)],
+                    self.gone.at[0], self.near_r.at[2 * q + g], at_tp(2 * y + other),
+                ).start()
+
+        def near_wait(self, q, g):
+            there = self.pair.at[0 : len((soon, rest)[g]), self.at(q)]
+            sem = self.near_r.at[2 * q + g]
+            remote(there, there, sem, sem, at_tp(t)).wait_recv()
+
+        def chip_sum(self, d, q):
+            chip = along(d)
+            mine = self.part[chip, c, self.at(q)].astype(F32)
+            return mine + self.pair[chip, self.at(q)].astype(F32)
+
+        def copy(self, line, q, to):
+            return remote(
+                self.send.at[line, self.at(q)], self.recv.at[line, self.at(q)], self.gone.at[1],
+                self.far_r.at[line * CHUNKS + q], at_tp(2 * along(to) + c),
             )
-            near[k].start()
-        for k in far_first:
-            chip = lax.rem(y + k, ny)
-            near[k].wait_recv()
-            send[chip] = (part[chip, c].astype(F32) + pair[chip].astype(F32)).astype(BF16)
-            remote(send.at[chip], recv.at[k], y_r.at[1], y_r.at[0], at_tp(2 * chip + c)).start()
-        near[0].wait_recv()
-        total = part[y, c].astype(F32) + pair[y].astype(F32)
-        if far_first:
-            there = recv.at[1:ny]
-            remote(there, there, y_r.at[1], y_r.at[0], at_tp(t)).wait_recv()
-            for k in far_first:
-                total = total + recv[k].astype(F32)
-        return total
-
-    def sums_left(part, recv, d_r, y_r):
-        remote(part.at[:, 0], part.at[:, 0], d_r.at[ny], d_r.at[ny], at_tp(t)).wait_send()
-        if far_first:
-            there = recv.at[1:ny]
-            remote(there, there, y_r.at[1], y_r.at[0], at_tp(t)).wait_send()
+
+        def go(self, line, q, to, value):
+            self.send[line, self.at(q)] = value.astype(BF16)
+            self.copy(line, q, to).start()
+
+        def got(self, line, q):
+            self.copy(line, q, 1).wait_recv()
+            return self.recv[line, self.at(q)].astype(F32)
+
+        def leg1(self, q):
+            self.near_wait(q, 0)
+            self.go(2, q, -2 * sigma_of(q), self.chip_sum(4, q))
+            for i, sigma in enumerate((1, -1)):
+                self.go(i, q, -sigma, self.chip_sum(-3 * sigma, q))
+
+        def neighbours(self, q):
+            self.near_wait(q, 1)
+            for i, sigma in enumerate((1, -1)):
+                self.go(3 + i, q, sigma, self.chip_sum(sigma, q))
+
+        def leg2(self, q):
+            for i, sigma in enumerate((1, -1)):
+                value = self.chip_sum(-2 * sigma, q) + self.got(i, q)
+                if sigma == sigma_of(q):
+                    value = value + self.got(2, q)
+                self.go(5 + i, q, -2 * sigma, value)
+
+        def total(self, q):
+            value = self.chip_sum(0, q)
+            for line in (3, 4, 5, 6):
+                value = value + self.got(line, q)
+            return value
+
+        def all_gone(self):
+            there = self.part.at[:, 0]
+            remote(there, there, self.gone.at[0], self.gone.at[0], at_tp(t)).wait_send()
+            remote(
+                self.send, self.send, self.gone.at[1], self.gone.at[1], at_tp(t)
+            ).wait_send()
 
     def tell(stat, sems, line):
         stat[t] = line
@@ -291,15 +345,23 @@
 
     scaled_in = ALPHA * vm["incoming"][...].astype(F32)
     row_sum = jnp.sum(scaled_in, -1, keepdims=True)
-    for k in far_first + [0]:
-        chip = lax.rem(y + k, ny)
-        at = pl.ds(pl.multiple_of(chip * 2 * width, 2 * width), 2 * width)
-        product = mm(heads_out, vm["final"][:, at])
-        part1[chip, 0] = product[:, :width].astype(BF16)
-        part1[chip, 1] = product[:, width:].astype(BF16)
-        row_sum = row_sum + jnp.sum(product, -1, keepdims=True)
+    first_tp = TpSum(part1, pair1, send1, recv1, near1_r, far1_r, gone1_s, rows // CHUNKS)
+    for g, group in enumerate((soon, rest)):
+        for d in group:
+            at = pl.ds(pl.multiple_of(along(d) * 2 * width, 2 * width), 2 * width)
+            product = mm(heads_out, vm["final"][:, at])
+            first_tp.put(d, slice(0, rows), product)
+            row_sum = row_sum + jnp.sum(product, -1, keepdims=True)
+        for q in range(CHUNKS):
+            first_tp.near(q, g)
+    for q in range(CHUNKS):
+        first_tp.leg1(q)
     tell(stat0, mean_s, to_row(row_sum))
-    projected = scattered_sum(part1, pair1, send1, recv1, d1_r, y1_r)
+    for q in range(CHUNKS):
+        first_tp.neighbours(q)
+    for q in range(CHUNKS):
+        first_tp.leg2(q)
+    projected = jnp.concatenate([first_tp.total(q) for q in range(CHUNKS)], axis=0)
     features = width * n_tp
     mean = to_col(heard_all(stat0, mean_s) / features)
     centred = scaled_in + projected - mean
@@ -332,39 +394,30 @@
     own_rows = jnp.dot(compact, came, preferred_element_type=F32).astype(BF16)
 
     lanes = pl.ds(pl.multiple_of(c * width, width), width)
-    turn = 1 - 2 * c
-    ahead = lax.rem(y + turn + ny, ny)
-    behind = lax.rem(y - turn + ny, ny)
-    most, least = ny // 2, (ny - 1) // 2
     piece_rows = slots // CHUNKS
 
     def rows_of(q):
         return slice(q * piece_rows, (q + 1) * piece_rows)
 
-    def along(d):
-        return lax.rem(y + d * turn + 2 * ny, ny)
-
     gathered[y, :, lanes] = own_rows
 
     def block(chip, q):
         return gathered.at[chip, rows_of(q), lanes]
 
-    def passed(chip, q, sem, to):
-        there = block(chip, q)
-        return remote(there, there, gone_s.at[1], sem, at_tp(2 * to + c))
-
-    def big(k, q, origin):
-        return passed(along(-origin), q, big_r.at[k * CHUNKS + q], ahead)
-
-    def small(k, q, origin):
-        return passed(along(origin), q, small_r.at[k * CHUNKS + q], behind)
-
-    def chips_at(k):
-        return [along(k)] if k == 0 or k > least else [along(-k), along(k)]
+    chips_of = ((0,), (2, -2), (1, -1), (3, -3, 4))
+
+    def passed(d, q, to, line):
+        there = block(along(d), q)
+        return remote(
+            there, there, gone_s.at[1], wire_r.at[line * CHUNKS + q], at_tp(2 * along(to) + c)
+        )
+
+    def came(d, q, line):
+        passed(d, q, 1, line).wait_recv()
 
     def hand(k, q):
-        for chip in reversed(chips_at(k)):
-            there = block(chip, q)
+        for d in chips_of[k]:
+            there = block(along(d), q)
             remote(
                 there, there, gone_s.at[0], own_r.at[k * CHUNKS + q], at_tp(2 * y + other)
             ).start()
@@ -374,7 +427,7 @@
         remote(there, there, sem, sem, at_tp(t)).wait_recv()
 
     def absorb(k, q):
-        chips, at_rows = chips_at(k), rows_of(q)
+        chips, at_rows = [along(d) for d in chips_of[k]], rows_of(q)
         wait_bytes(len(chips), own_r.at[k * CHUNKS + q])
         for chip in chips:
             block_in = gathered[chip, at_rows, :]
@@ -403,11 +456,9 @@
 
         return noted(0), noted(1), noted(2) + noted(3)
 
-    for q in range(CHUNKS):
-        if most:
-            big(0, q, 0).start()
-        if least:
-            small(0, q, 0).start()
+    for line, d in enumerate((2, -2, 1, -1)):
+        for q in range(CHUNKS):
+            passed(0, q, d, line).start()
     for q in range(CHUNKS):
         hand(0, q)
     row_scale = lax.rsqrt(heard_all(stat1, sq1_s) / features + 1e-05)
@@ -418,24 +469,28 @@
     told[:, 3:4, :] = (scales - coarse.astype(F32)).astype(BF16)
     scatter(told, heard, note_s)
     middle = (centred * to_col(row_scale) * vm["gain1"][...]).astype(BF16)
-    waiting = [(0, q) for q in range(CHUNKS)]
-    slot_notes = None
-    for k in range(1, most + 1):
-        for q in range(CHUNKS):
-            big(k - 1, q, k).wait_recv()
-            if k < most:
-                big(k, q, k).start()
-            if k <= least:
-                small(k - 1, q, k).wait_recv()
-                if k < least:
-                    small(k, q, k).start()
-            hand(k, q)
-            absorb(*waiting.pop(0))
-            waiting.append((k, q))
-        if k == most - 1:
-            slot_notes = all_noted()
-    if slot_notes is None:
-        slot_notes = all_noted()
+    for q in range(CHUNKS):
+        for line, sigma in enumerate((1, -1)):
+            came(-2 * sigma, q, line)
+            passed(-2 * sigma, q, sigma, 4 + line).start()
+            if sigma == sigma_of(q):
+                passed(-2 * sigma, q, 2 * sigma, 6).start()
+        hand(1, q)
+    for q in range(CHUNKS):
+        absorb(0, q)
+    for q in range(CHUNKS):
+        for line, sigma in enumerate((1, -1)):
+            came(-sigma, q, 2 + line)
+        hand(2, q)
+    for q in range(CHUNKS):
+        absorb(1, q)
+    slot_notes = all_noted()
+    for q in range(CHUNKS):
+        for line, sigma in enumerate((1, -1)):
+            came(-3 * sigma, q, 4 + line)
+        came(4, q, 6)
+        hand(3, q)
+        absorb(2, q)
 
     def expert(q):
         at_rows = rows_of(q)
@@ -445,66 +500,27 @@
         )
         common = acc_s[at_rows] * scale
         shared = (silu(common[:, :sf]) * common[:, sf:] * flag).astype(BF16)
-        for chip in range(ny):
-            at = slice(chip * 2 * width, (chip + 1) * 2 * width)
-            product = jnp.dot(hidden, vm["lower"][:, at], preferred_element_type=F32) + jnp.dot(
-                shared, vm["common_low"][:, at], preferred_element_type=F32
-            )
-            part2[chip, 0, at_rows] = product[:, :width].astype(BF16)
-            part2[chip, 1, at_rows] = product[:, width:].astype(BF16)
-        for g, group in enumerate(groups):
+        for g, group in enumerate((soon, rest)):
             for d in group:
-                chip = along(d)
-                remote(
-                    part2.at[chip, other, at_rows], pair2.at[chip, at_rows], gone_s.at[2],
-                    near_r.at[2 * q + g], at_tp(2 * y + other),
-                ).start()
-
-    soon = sorted({most % ny, least % ny, -least % ny} - {0})
-    groups = [soon, [d for d in range(ny) if d not in soon]]
-    for q in range(CHUNKS):
-        absorb(*waiting.pop(0))
+                at = pl.ds(pl.multiple_of(along(d) * 2 * width, 2 * width), 2 * width)
+                product = jnp.dot(hidden, vm["lower"][:, at], preferred_element_type=F32) + jnp.dot(
+                    shared, vm["common_low"][:, at], preferred_element_type=F32
+                )
+                second_tp.put(d, at_rows, product)
+            second_tp.near(q, g)
+
+    second_tp = TpSum(part2, pair2, send2, recv2, near2_r, far2_r, gone2_s, piece_rows)
+    for q in range(CHUNKS):
+        absorb(3, q)
         expert(q)
-
-    def chip_sum(d, q):
-        chip, at_rows = along(d), rows_of(q)
-        return part2[chip, c, at_rows].astype(F32) + pair2[chip, at_rows].astype(F32)
-
-    def ring_step(j, q, reach, sign, send, recv, sem, gone, to):
-        at_rows = rows_of(q)
-        value = chip_sum(sign * (reach - j), q)
-        if j:
-            came_in(j - 1, q, send, recv, sem, gone, to).wait_recv()
-            value = value + recv[j - 1, at_rows].astype(F32)
-        send[j, at_rows] = value.astype(BF16)
-        came_in(j, q, send, recv, sem, gone, to).start()
-
-    def came_in(j, q, send, recv, sem, gone, to):
-        at_rows = rows_of(q)
-        return remote(
-            send.at[j, at_rows], recv.at[j, at_rows], gone, sem.at[j * CHUNKS + q],
-            at_tp(2 * to + c),
-        )
-
-    large = (send2, recv2, far_r, gone_s.at[3], ahead)
-    little = (send3, recv3, back_r, gone_s.at[4], behind)
-    for j in range(most):
-        for q in range(CHUNKS):
-            if j < 2 and groups[j]:
-                wait_bytes(len(groups[j]), near_r.at[2 * q + j])
-            ring_step(j, q, most, 1, *large)
-            if j < least:
-                ring_step(j, q, least, -1, *little)
-    for q in range(CHUNKS):
-        if most < 2:
-            wait_bytes(len(groups[1]), near_r.at[2 * q + 1])
-        value = chip_sum(0, q)
-        if most:
-            came_in(most - 1, q, *large).wait_recv()
-            value = value + recv2[most - 1, rows_of(q)].astype(F32)
-        if least:
-            came_in(least - 1, q, *little).wait_recv()
-            value = value + recv3[least - 1, rows_of(q)].astype(F32)
+    for q in range(CHUNKS):
+        second_tp.leg1(q)
+    for q in range(CHUNKS):
+        second_tp.neighbours(q)
+    for q in range(CHUNKS):
+        second_tp.leg2(q)
+    for q in range(CHUNKS):
+        value = second_tp.total(q)
         share_sp = n_sp // CHUNKS
         owners = slice(q * share_sp, (q + 1) * share_sp)
         spots = slice(q * share_sp * stride, (q + 1) * share_sp * stride)
@@ -531,11 +547,9 @@
     totals = heard_all(stat2, sq2_s) / features
     mean2, square2 = totals[0:1, :], totals[1:2, :]
     scale2 = lax.rsqrt(square2 - mean2 * mean2 + 1e-05)
-    out_vm[...] = (
+    out_ref[...] = (
         (second_sum - to_col(mean2)) * to_col(scale2) * vm["gain2"][...]
     ).astype(BF16)
-    out_copy = pltpu.make_async_copy(out_vm, out_hbm, out_sem)
-    out_copy.start()
 
     for copy in first:
         copy.wait_send()
@@ -544,14 +558,9 @@
         remote(there, there, sem, sem, at_tp(t)).wait_send()
 
     all_gone(pair2, gone_s.at[0])
-    all_gone(pair2, gone_s.at[2])
-    if most:
-        all_gone(pair2.at[1:ny], gone_s.at[1])
-        all_gone(send2, gone_s.at[3])
-    if least:
-        all_gone(send3, gone_s.at[4])
-    sums_left(part1, recv1, d1_r, y1_r)
-    out_copy.wait()
+    all_gone(pair2.at[1:ny], gone_s.at[1])
+    first_tp.all_gone()
+    second_tp.all_gone()
 
 
 def dims_names():
@@ -576,7 +585,6 @@
     slots = n_sp * cap
     ff, features = valve.shape[2], valve.shape[1]
     sf = common_valve.shape[1]
-    most, least = max(1, ny // 2), max(1, (ny - 1) // 2)
     dims = (n_sp, n_tp, rows, experts, cap, stride)
     args = {
         "probe": probe, "address": address, "content": content, "storage": storage,
@@ -601,26 +609,26 @@
     return pl.pallas_call(
         functools.partial(kernel, dims),
         out_shape=jax.ShapeDtypeStruct((rows, width), BF16),
-        in_specs=[pl.BlockSpec(memory_space=pl.ANY)] * len(operands),
-        out_specs=pl.BlockSpec(memory_space=pl.ANY),
+        in_specs=[pl.BlockSpec(memory_space=pltpu.HBM)] * len(operands),
+        out_specs=pl.BlockSpec(memory_space=pltpu.VMEM),
         scratch_shapes=own
         + [
             vmem(2 * width + 16, width), vmem(REACH, 2 * width + 16, width),
             vmem(width, width), vmem(width, width),
-            vmem(ny, 2, rows, width), vmem(ny, rows, width), vmem(ny, rows, width),
-            vmem(ny, rows, width),
+            vmem(ny, 2, rows, width), vmem(ny, rows, width), vmem(7, rows, width),
+            vmem(7, rows, width),
             vmem(n_tp, 1, rows, kind=F32), vmem(n_tp, 1, rows, kind=F32),
             vmem(n_tp, 2, rows, kind=F32),
             vmem(n_sp, stride, width), vmem(n_sp, stride, width),
             vmem(n_sp, 16, width), vmem(n_sp, 16, width),
             vmem(ny, slots, 2 * width), vmem(2, slots, ff, kind=F32), vmem(slots, 2 * sf, kind=F32),
-            vmem(ny, 2, slots, width), vmem(ny, slots, width), vmem(most, slots, width),
-            vmem(most, slots, width), vmem(least, slots, width), vmem(least, slots, width),
-            vmem(n_sp, stride, width), vmem(n_sp, stride, width), vmem(rows, width),
-            dma((len(operands),)), dma, dma((REACH,)), dma((REACH,)), dma((2,)),
-            dma((ny + 1,)), dma((2,)), dma((2,)), dma((2,)), dma((2,)),
-            dma((2,)), dma((2,)), dma((2,)), dma((most * CHUNKS,)), dma((least * CHUNKS,)), dma(((most + 1) * CHUNKS,)), dma((5,)),
-            dma((2 * CHUNKS,)), dma((most * CHUNKS,)), dma((least * CHUNKS,)),
+            vmem(ny, 2, slots, width), vmem(ny, slots, width), vmem(7, slots, width),
+            vmem(7, slots, width),
+            vmem(n_sp, stride, width), vmem(n_sp, stride, width),
+            dma((len(operands),)), dma((REACH,)), dma((REACH,)), dma((2,)),
+            dma((2 * CHUNKS,)), dma((7 * CHUNKS,)), dma((2,)), dma((2,)), dma((2,)), dma((2,)),
+            dma((2,)), dma((2,)), dma((2,)), dma((7 * CHUNKS,)), dma((4 * CHUNKS,)), dma((2,)),
+            dma((2 * CHUNKS,)), dma((7 * CHUNKS,)), dma((2,)),
         ],
         compiler_params=pltpu.CompilerParams(
             collective_id=0, has_side_effects=True, vmem_limit_bytes=60 * 1024 * 1024

time: 88.5 us -> 82.1 us (0.928)
  Pallas kernels: 86.3 us -> 79.8 us
    pallas_call x1, Pallas kernels: 86.3 us -> 79.8 us  [shards(): pl.pallas_call(functools.partial(kernel, dims), out_shape=jax.ShapeDtypeS...]
where the time goes in v4:
time: 82.1 us; the launch traced here: 81.9 us
  Pallas kernels  79.8 us (97%)
  local copies, waits for them, and re-layouts  1.38 us (2%)
    pallas_call x1, Pallas kernels, shards(): pl.pallas_call(functools.partial(kernel, dims), out_shape=jax.ShapeDtypeS...  79.8 us

profile of v4, /device:TPU:1, one launch (start us, length us, event | category | flops | bytes accessed | tf_op | source)
XLA Modules:
  0.0 81.9 jit_solution(3164841632636170779)
XLA Ops:
  0.7 79.8 %layer.1 = bf16[128,128]{1,0:T(8,128)(2,1)} custom-call(bf16[128,128]{1,0:T(8,128)(2,1)} %refs_0_.1, bf16[128,128]{1,0:T(8,128)(2,1)} %refs_1_.1, bf16[128,128]{1,0:T(8,128)(2,1)} %refs_2_.1, f32[1,128]{1,0:T(1,128)} %refs_3_.1, f32[1,128]{1,0:T(1,128)} %refs_4_.1, f32[1,128]{1,0:T(1,128)} %refs_5_.1, s32[1,128]{1,0:T(1,128)} %bitcast.18, ...), custom_call_target="tpu_custom_call" | custom-call | tf_op jit(solution)/shard_map/layer/pallas_call | solution.py:609
  80.5 1.4 %copy.24 = bf16[128,128]{1,0:T(8,128)(2,1)} copy(bf16[128,128]{1,0:T(8,128)(2,1)} %layer.1) | data formatting | bytes 65536

commit v5 on v4

--- a/solution.py
+++ b/solution.py
@@ -56,7 +56,7 @@
         stat0, stat1, stat2,
         sent, arrived, told, heard, gathered, acc_g, acc_s,
         part2, pair2, send2, recv2,
-        rsend, returned,
+        rsend, returned, undo, widen,
         load_sem, pa_s, pa_r, pb_s,
         near1_r, far1_r, gone1_s, mean_s, sq1_s, sq2_s,
         dis_s, note_s, ret_s, wire_r, own_r, gone_s,
@@ -83,20 +83,25 @@
 
     barrier = pltpu.get_barrier_semaphore()
 
-    def greet_sp(k, carry):
+    nx = 4
+    nz = n_sp // nx
+    hops = sorted(
+        ((dz, dx) for dz in range(nz) for dx in range(nx) if dz or dx),
+        key=lambda d: -min(d[0], nz - d[0]) - min(d[1], nx - d[1]),
+    )
+    z, x = s // nx, lax.rem(s, nx)
+
+    def beside(dz, dx):
+        return lax.rem(z + dz, nz) * nx + lax.rem(x + dx, nx)
+
+    for dz, dx in hops:
         pl.semaphore_signal(
-            barrier, inc=1, device_id=at_sp(lax.rem(s + k, n_sp)), device_id_type=MESH
+            barrier, inc=1, device_id=at_sp(beside(dz, dx)), device_id_type=MESH
         )
-        return carry
-
-    def greet_tp(k, carry):
+    for k in sorted(range(1, n_tp), key=lambda k: -min(k, n_tp - k)):
         pl.semaphore_signal(
             barrier, inc=1, device_id=at_tp(lax.rem(t + k, n_tp)), device_id_type=MESH
         )
-        return carry
-
-    lax.fori_loop(1, n_sp, greet_sp, 0)
-    lax.fori_loop(1, n_tp, greet_tp, 0)
     sf = vm["common"].shape[0] // 2
     loads = {}
     for k, name in enumerate(names):
@@ -203,6 +208,7 @@
     wide = mm(spread, jnp.concatenate([coded, shares, to0], axis=1))
     hot = wide[:, :rows] == (place + 1).astype(F32)
     dispatch = hot.astype(BF16)
+    undo[...] = hot.astype(F32).T.astype(BF16)
     slot_share = jnp.sum(jnp.where(hot, wide[:, rows : 2 * rows], 0.0), axis=1, keepdims=True)
     slot_first = jnp.sum(jnp.where(hot, wide[:, 2 * rows :], 0.0), axis=1, keepdims=True)
     here = (iota((padded, rows), 1) == place).astype(F32)
@@ -218,6 +224,12 @@
     within = compact_i - source * cap
     column = iota((slots, padded), 1).astype(F32)
     compact = (column == source * stride + within).astype(BF16)
+    open_i = iota((padded, slots), 1).astype(F32)
+    open_source = jnp.floor((open_i + 0.5) * (1.0 / cap))
+    spread_out = (
+        iota((padded, slots), 0).astype(F32) == open_source * (stride - cap) + open_i
+    ).astype(BF16)
+    widen[...] = spread_out
     slot_lane = iota((slots, rows), 1).astype(F32) == within[:, :rows]
     valve = silu(vm["exit"][...].astype(F32))
 
@@ -242,9 +254,10 @@
         carry_out, carry_in, pb_s.at[0], pb_s.at[1], at_sp(lax.rem(s + REACH, n_sp))
     )
     second.start()
+    from_carry = mm(q_grown, map12).astype(BF16)
+    known = own_mixed + mm(q_grown, shift12) * joined
     second.wait_recv()
-    incoming = (shift12 + mm(map12, carry_in[...])) * joined
-    mixed = own_mixed + mm(q_grown, incoming)
+    mixed = known + mm(from_carry, carry_in[...]) * joined
     scaled = mixed * lax.rsqrt(jnp.mean(mixed * mixed, -1, keepdims=True) + 1e-06)
     heads_out = (scaled * valve).astype(BF16)
 
@@ -366,24 +379,25 @@
     mean = to_col(heard_all(stat0, mean_s) / features)
     centred = scaled_in + projected - mean
 
-    nx = 4
-    nz = n_sp // nx
-    hops = sorted(
-        ((dz, dx) for dz in range(nz) for dx in range(nx) if dz or dx),
-        key=lambda d: -min(d[0], nz - d[0]) - min(d[1], nx - d[1]),
-    )
+    sent_rows = -(-cap // 2) * 2
+
+    def scattered(src, dst, sems, to):
+        top = min(src.shape[1], sent_rows)
+        return remote(
+            src.at[to, 0:top], dst.at[s, 0:top], sems.at[0], sems.at[1], at_sp(to)
+        )
 
     def scatter(src, dst, sems):
-        z, x = s // nx, lax.rem(s, nx)
         for dz, dx in hops:
-            to = lax.rem(z + dz, nz) * nx + lax.rem(x + dx, nx)
-            remote(src.at[to], dst.at[s], sems.at[0], sems.at[1], at_sp(to)).start()
+            scattered(src, dst, sems, beside(dz, dx)).start()
         dst[s] = src[s]
 
     def collected(dst, sems):
-        there = dst.at[1:n_sp]
+        top = min(dst.shape[1], sent_rows)
+        there = dst.at[1:n_sp, 0:top]
         remote(there, there, sems.at[0], sems.at[1], at_sp(s)).wait()
-        return dst[...].reshape(dst.shape[0] * dst.shape[1], dst.shape[2])
+        came = jnp.where(iota(dst.shape, 1) < top, dst[...].astype(F32), 0.0).astype(BF16)
+        return came.reshape(dst.shape[0] * dst.shape[1], dst.shape[2])
 
     gained = (centred * vm["gain1"][...]).astype(BF16)
     payload = jnp.dot(dispatch, gained, preferred_element_type=F32)
@@ -429,20 +443,21 @@
     def absorb(k, q):
         chips, at_rows = [along(d) for d in chips_of[k]], rows_of(q)
         wait_bytes(len(chips), own_r.at[k * CHUNKS + q])
+        gates = ups = common = 0.0
         for chip in chips:
             block_in = gathered[chip, at_rows, :]
             at = pl.ds(pl.multiple_of(chip * 2 * width, 2 * width), 2 * width)
-            gates = jnp.dot(block_in, vm["valve"][at, :], preferred_element_type=F32)
-            ups = jnp.dot(block_in, vm["raise"][at, :], preferred_element_type=F32)
-            common = lax.dot_general(
+            gates += jnp.dot(block_in, vm["valve"][at, :], preferred_element_type=F32)
+            ups += jnp.dot(block_in, vm["raise"][at, :], preferred_element_type=F32)
+            common += lax.dot_general(
                 block_in, vm["common"][:, at], (((1,), (1,)), ((), ())), preferred_element_type=F32
             )
-            if k == 0:
-                acc_g[0, at_rows], acc_g[1, at_rows], acc_s[at_rows] = gates, ups, common
-            else:
-                acc_g[0, at_rows] += gates
-                acc_g[1, at_rows] += ups
-                acc_s[at_rows] += common
+        if k:
+            gates, ups = gates + acc_g[0, at_rows], ups + acc_g[1, at_rows]
+            common = common + acc_s[at_rows]
+        if k < 3:
+            acc_g[0, at_rows], acc_g[1, at_rows], acc_s[at_rows] = gates, ups, common
+        return gates, ups, common
 
     def all_noted():
         notes = collected(heard, note_s)
@@ -492,13 +507,11 @@
         hand(3, q)
         absorb(2, q)
 
-    def expert(q):
+    def expert(q, gates, ups, common):
         at_rows = rows_of(q)
         weight, flag, scale = (v[at_rows] for v in slot_notes)
-        hidden = (silu(acc_g[0, at_rows] * scale) * acc_g[1, at_rows] * (scale * weight)).astype(
-            BF16
-        )
-        common = acc_s[at_rows] * scale
+        hidden = (silu(gates * scale) * ups * (scale * weight)).astype(BF16)
+        common = common * scale
         shared = (silu(common[:, :sf]) * common[:, sf:] * flag).astype(BF16)
         for g, group in enumerate((soon, rest)):
             for d in group:
@@ -511,8 +524,7 @@
 
     second_tp = TpSum(part2, pair2, send2, recv2, near2_r, far2_r, gone2_s, piece_rows)
     for q in range(CHUNKS):
-        absorb(3, q)
-        expert(q)
+        expert(q, *absorb(3, q))
     for q in range(CHUNKS):
         second_tp.leg1(q)
     for q in range(CHUNKS):
@@ -525,7 +537,7 @@
         owners = slice(q * share_sp, (q + 1) * share_sp)
         spots = slice(q * share_sp * stride, (q + 1) * share_sp * stride)
         rsend[owners] = (
-            mm_tn(compact[rows_of(q), spots], value)
+            mm(widen[spots, rows_of(q)], value)
             .astype(BF16)
             .reshape(share_sp, stride, rows)
         )
@@ -534,13 +546,11 @@
 
             @pl.when(to != s)
             def _(to=to):
-                remote(
-                    rsend.at[to], returned.at[s], ret_s.at[0], ret_s.at[1], at_sp(to)
-                ).start()
+                scattered(rsend, returned, ret_s, to).start()
 
     returned[s] = rsend[s]
     back = collected(returned, ret_s)
-    mixture = mm_tn(dispatch, back)
+    mixture = mm(undo[...], back)
     second_sum = ALPHA * middle.astype(F32) + mixture
     sums = [jnp.sum(v, -1, keepdims=True) for v in (second_sum, second_sum * second_sum)]
     tell(stat2, sq2_s, jnp.concatenate([to_row(v) for v in sums], axis=0))
@@ -620,11 +630,12 @@
             vmem(n_tp, 1, rows, kind=F32), vmem(n_tp, 1, rows, kind=F32),
             vmem(n_tp, 2, rows, kind=F32),
             vmem(n_sp, stride, width), vmem(n_sp, stride, width),
-            vmem(n_sp, 16, width), vmem(n_sp, 16, width),
+            vmem(n_sp, 8, width), vmem(n_sp, 8, width),
             vmem(ny, slots, 2 * width), vmem(2, slots, ff, kind=F32), vmem(slots, 2 * sf, kind=F32),
             vmem(ny, 2, slots, width), vmem(ny, slots, width), vmem(7, slots, width),
             vmem(7, slots, width),
             vmem(n_sp, stride, width), vmem(n_sp, stride, width),
+            vmem(rows, n_sp * stride), vmem(n_sp * stride, slots),
             dma((len(operands),)), dma((REACH,)), dma((REACH,)), dma((2,)),
             dma((2 * CHUNKS,)), dma((7 * CHUNKS,)), dma((2,)), dma((2,)), dma((2,)), dma((2,)),
             dma((2,)), dma((2,)), dma((2,)), dma((7 * CHUNKS,)), dma((4 * CHUNKS,)), dma((2,)),

time: 82.1 us -> 80.9 us (0.985)
  Pallas kernels: 79.8 us -> 78.7 us
    pallas_call x1, Pallas kernels: 79.8 us -> 78.7 us  [shards(): pl.pallas_call(functools.partial(kernel, dims), out_shape=jax.ShapeDtypeS...]
where the time goes in v5:
time: 80.9 us; the launch traced here: 80.7 us
  Pallas kernels  78.7 us (97%)
  local copies, waits for them, and re-layouts  1.38 us (2%)
    pallas_call x1, Pallas kernels, shards(): pl.pallas_call(functools.partial(kernel, dims), out_shape=jax.ShapeDtypeS...  78.7 us

profile of v5, /device:TPU:1, one launch (start us, length us, event | category | flops | bytes accessed | tf_op | source)
XLA Modules:
  0.0 80.7 jit_solution(3651398730836075878)
XLA Ops:
  0.7 78.7 %layer.1 = bf16[128,128]{1,0:T(8,128)(2,1)} custom-call(bf16[128,128]{1,0:T(8,128)(2,1)} %refs_0_.1, bf16[128,128]{1,0:T(8,128)(2,1)} %refs_1_.1, bf16[128,128]{1,0:T(8,128)(2,1)} %refs_2_.1, f32[1,128]{1,0:T(1,128)} %refs_3_.1, f32[1,128]{1,0:T(1,128)} %refs_4_.1, f32[1,128]{1,0:T(1,128)} %refs_5_.1, s32[1,128]{1,0:T(1,128)} %bitcast.18, ...), custom_call_target="tpu_custom_call" | custom-call | tf_op jit(solution)/shard_map/layer/pallas_call | solution.py:619
  79.3 1.4 %copy.24 = bf16[128,128]{1,0:T(8,128)(2,1)} copy(bf16[128,128]{1,0:T(8,128)(2,1)} %layer.1) | data formatting | bytes 65536

commit v6 on v5

--- a/solution.py
+++ b/solution.py
@@ -303,15 +303,19 @@
         def copy(self, line, q, to):
             return remote(
                 self.send.at[line, self.at(q)], self.recv.at[line, self.at(q)], self.gone.at[1],
-                self.far_r.at[line * CHUNKS + q], at_tp(2 * along(to) + c),
+                self.far_r.at[(line > 2) * CHUNKS + q], at_tp(2 * along(to) + c),
             )
 
         def go(self, line, q, to, value):
             self.send[line, self.at(q)] = value.astype(BF16)
             self.copy(line, q, to).start()
 
+        def got_all(self, first, last, q):
+            there = self.recv.at[first:last, self.at(q)]
+            sem = self.far_r.at[(first > 2) * CHUNKS + q]
+            remote(there, there, sem, sem, at_tp(t)).wait_recv()
+
         def got(self, line, q):
-            self.copy(line, q, 1).wait_recv()
             return self.recv[line, self.at(q)].astype(F32)
 
         def leg1(self, q):
@@ -326,6 +330,7 @@
                 self.go(3 + i, q, sigma, self.chip_sum(sigma, q))
 
         def leg2(self, q):
+            self.got_all(0, 3, q)
             for i, sigma in enumerate((1, -1)):
                 value = self.chip_sum(-2 * sigma, q) + self.got(i, q)
                 if sigma == sigma_of(q):
@@ -334,6 +339,7 @@
 
         def total(self, q):
             value = self.chip_sum(0, q)
+            self.got_all(3, 7, q)
             for line in (3, 4, 5, 6):
                 value = value + self.got(line, q)
             return value
@@ -347,7 +353,7 @@
 
     def tell(stat, sems, line):
         stat[t] = line
-        for k in range(1, n_tp):
+        for k in sorted(range(1, n_tp), key=lambda k: -min(k, n_tp - k)):
             to = lax.rem(t + k, n_tp)
             remote(stat.at[t], stat.at[t], sems.at[0], sems.at[1], at_tp(to)).start()
 
@@ -396,8 +402,12 @@
         top = min(dst.shape[1], sent_rows)
         there = dst.at[1:n_sp, 0:top]
         remote(there, there, sems.at[0], sems.at[1], at_sp(s)).wait()
-        came = jnp.where(iota(dst.shape, 1) < top, dst[...].astype(F32), 0.0).astype(BF16)
-        return came.reshape(dst.shape[0] * dst.shape[1], dst.shape[2])
+        return as_rows(dst[...], top)
+
+    def as_rows(came, top):
+        shape = came.shape
+        came = jnp.where(iota(shape, 1) < top, came.astype(F32), 0.0).astype(BF16)
+        return came.reshape(shape[0] * shape[1], shape[2])
 
     gained = (centred * vm["gain1"][...]).astype(BF16)
     payload = jnp.dot(dispatch, gained, preferred_element_type=F32)
@@ -405,29 +415,21 @@
     scatter(sent, arrived, dis_s)
     tell(stat1, sq1_s, to_row(jnp.sum(centred * centred, -1, keepdims=True)))
     came = collected(arrived, dis_s)
-    own_rows = jnp.dot(compact, came, preferred_element_type=F32).astype(BF16)
-
     lanes = pl.ds(pl.multiple_of(c * width, width), width)
     piece_rows = slots // CHUNKS
 
     def rows_of(q):
         return slice(q * piece_rows, (q + 1) * piece_rows)
 
-    gathered[y, :, lanes] = own_rows
-
     def block(chip, q):
         return gathered.at[chip, rows_of(q), lanes]
 
     chips_of = ((0,), (2, -2), (1, -1), (3, -3, 4))
 
-    def passed(d, q, to, line):
+    def passed(d, q, to, late):
         there = block(along(d), q)
-        return remote(
-            there, there, gone_s.at[1], wire_r.at[line * CHUNKS + q], at_tp(2 * along(to) + c)
-        )
-
-    def came(d, q, line):
-        passed(d, q, 1, line).wait_recv()
+        sem = wire_r.at[late * CHUNKS + q]
+        remote(there, there, gone_s.at[1], sem, at_tp(2 * along(to) + c)).start()
 
     def hand(k, q):
         for d in chips_of[k]:
@@ -471,9 +473,14 @@
 
         return noted(0), noted(1), noted(2) + noted(3)
 
-    for line, d in enumerate((2, -2, 1, -1)):
-        for q in range(CHUNKS):
-            passed(0, q, d, line).start()
+    for q in range(CHUNKS):
+        found = jnp.dot(compact[rows_of(q)], came, preferred_element_type=F32)
+        gathered[y, rows_of(q), lanes] = found.astype(BF16)
+        for sigma in (1, -1):
+            passed(0, q, 2 * sigma, 0)
+    for q in range(CHUNKS):
+        for sigma in (1, -1):
+            passed(0, q, sigma, 1)
     for q in range(CHUNKS):
         hand(0, q)
     row_scale = lax.rsqrt(heard_all(stat1, sq1_s) / features + 1e-05)
@@ -485,27 +492,26 @@
     scatter(told, heard, note_s)
     middle = (centred * to_col(row_scale) * vm["gain1"][...]).astype(BF16)
     for q in range(CHUNKS):
-        for line, sigma in enumerate((1, -1)):
-            came(-2 * sigma, q, line)
-            passed(-2 * sigma, q, sigma, 4 + line).start()
+        wait_bytes(2, wire_r.at[q])
+        for sigma in (1, -1):
             if sigma == sigma_of(q):
-                passed(-2 * sigma, q, 2 * sigma, 6).start()
+                passed(-2 * sigma, q, 2 * sigma, 2)
+            passed(-2 * sigma, q, sigma, 2)
         hand(1, q)
     for q in range(CHUNKS):
         absorb(0, q)
     for q in range(CHUNKS):
-        for line, sigma in enumerate((1, -1)):
-            came(-sigma, q, 2 + line)
+        wait_bytes(2, wire_r.at[CHUNKS + q])
         hand(2, q)
     for q in range(CHUNKS):
         absorb(1, q)
     slot_notes = all_noted()
     for q in range(CHUNKS):
-        for line, sigma in enumerate((1, -1)):
-            came(-3 * sigma, q, 4 + line)
-        came(4, q, 6)
+        wait_bytes(3, wire_r.at[2 * CHUNKS + q])
         hand(3, q)
-        absorb(2, q)
+        if q == 0:
+            for k in range(CHUNKS):
+                absorb(2, k)
 
     def expert(q, gates, ups, common):
         at_rows = rows_of(q)
@@ -523,10 +529,12 @@
             second_tp.near(q, g)
 
     second_tp = TpSum(part2, pair2, send2, recv2, near2_r, far2_r, gone2_s, piece_rows)
-    for q in range(CHUNKS):
-        expert(q, *absorb(3, q))
-    for q in range(CHUNKS):
-        second_tp.leg1(q)
+    expert(0, *absorb(3, 0))
+    for q in range(1, CHUNKS):
+        ready = absorb(3, q)
+        second_tp.leg1(q - 1)
+        expert(q, *ready)
+    second_tp.leg1(CHUNKS - 1)
     for q in range(CHUNKS):
         second_tp.neighbours(q)
     for q in range(CHUNKS):
@@ -606,7 +614,10 @@
         "common_low": common_lowering, "channel": channel[None, :],
     }
     names = dims_names()
-    operands = [args[n] for n in names]
+    operands = [
+        args[n] if n == "channel" else pltpu.with_memory_space_constraint(args[n], pltpu.HBM)
+        for n in names
+    ]
     dma = pltpu.SemaphoreType.DMA
     shapes = {n: a.shape for n, a in args.items()}
     shapes["common"] = (2 * sf, features)
@@ -637,12 +648,12 @@
             vmem(n_sp, stride, width), vmem(n_sp, stride, width),
             vmem(rows, n_sp * stride), vmem(n_sp * stride, slots),
             dma((len(operands),)), dma((REACH,)), dma((REACH,)), dma((2,)),
-            dma((2 * CHUNKS,)), dma((7 * CHUNKS,)), dma((2,)), dma((2,)), dma((2,)), dma((2,)),
-            dma((2,)), dma((2,)), dma((2,)), dma((7 * CHUNKS,)), dma((4 * CHUNKS,)), dma((2,)),
-            dma((2 * CHUNKS,)), dma((7 * CHUNKS,)), dma((2,)),
+            dma((2 * CHUNKS,)), dma((2 * CHUNKS,)), dma((2,)), dma((2,)), dma((2,)), dma((2,)),
+            dma((2,)), dma((2,)), dma((2,)), dma((3 * CHUNKS,)), dma((4 * CHUNKS,)),
+            dma((2,)), dma((2 * CHUNKS,)), dma((2 * CHUNKS,)), dma((2,)),
         ],
         compiler_params=pltpu.CompilerParams(
-            collective_id=0, has_side_effects=True, vmem_limit_bytes=60 * 1024 * 1024
+            collective_id=0, has_side_effects=True, vmem_limit_bytes=48 * 1024 * 1024
         ),
         name="layer",
     )(*operands)

time: 80.9 us -> 78.4 us (0.969)
  Pallas kernels: 78.7 us -> 77 us
    pallas_call x1, Pallas kernels: 78.7 us -> 77 us  [shards(): pl.pallas_call(functools.partial(kernel, dims), out_shape=jax.ShapeDtypeS...]
where the time goes in v6:
time: 78.4 us; the launch traced here: 78.3 us
  Pallas kernels  77 us (98%)
    pallas_call x1, Pallas kernels, shards(): pl.pallas_call(functools.partial(kernel, dims), out_shape=jax.ShapeDtypeS...  77 us

profile of v6, /device:TPU:1, one launch (start us, length us, event | category | flops | bytes accessed | tf_op | source)
XLA Modules:
  0.0 78.3 jit_solution(9780372056700112319)
XLA Ops:
  0.7 77.0 %layer.1 = bf16[128,128]{1,0:T(8,128)(2,1)S(1)} custom-call(bf16[128,128]{1,0:T(8,128)(2,1)} %refs_0_.1, bf16[128,128]{1,0:T(8,128)(2,1)} %refs_1_.1, bf16[128,128]{1,0:T(8,128)(2,1)} %refs_2_.1, f32[1,128]{1,0:T(1,128)} %refs_3_.1, f32[1,128]{1,0:T(1,128)} %refs_4_.1, f32[1,128]{1,0:T(1,128)} %refs_5_.1, s32[1,128]{1,0:T(1,128)} %bitcast.18, ...), custom_call_target="tpu_custom_call" | custom-call | tf_op jit(solution)/shard_map/layer/pallas_call | solution.py:630
  77.6 0.6 copy.24

commit v7 on v6

--- a/solution.py
+++ b/solution.py
@@ -94,14 +94,6 @@
     def beside(dz, dx):
         return lax.rem(z + dz, nz) * nx + lax.rem(x + dx, nx)
 
-    for dz, dx in hops:
-        pl.semaphore_signal(
-            barrier, inc=1, device_id=at_sp(beside(dz, dx)), device_id_type=MESH
-        )
-    for k in sorted(range(1, n_tp), key=lambda k: -min(k, n_tp - k)):
-        pl.semaphore_signal(
-            barrier, inc=1, device_id=at_tp(lax.rem(t + k, n_tp)), device_id_type=MESH
-        )
     sf = vm["common"].shape[0] // 2
     loads = {}
     for k, name in enumerate(names):
@@ -114,6 +106,14 @@
     early = ("probe", "address", "content", "storage", "fade", "extra", "channel", "label")
     for name in early:
         loads[name].start()
+    for dz, dx in hops:
+        pl.semaphore_signal(
+            barrier, inc=1, device_id=at_sp(beside(dz, dx)), device_id_type=MESH
+        )
+    for k in sorted(range(1, n_tp), key=lambda k: -min(k, n_tp - k)):
+        pl.semaphore_signal(
+            barrier, inc=1, device_id=at_tp(lax.rem(t + k, n_tp)), device_id_type=MESH
+        )
     for name in names:
         if name not in early:
             loads[name].start()
@@ -187,7 +187,7 @@
         )
         for k, top in enumerate(tops)
     ]
-    for k in reversed(range(REACH)):
+    for k in (1, 2, 0):
         first[k].start()
 
     for name in names:

time: 78.4 us -> 78.6 us (level)
  no operation moved by 1% of the time
where the time goes in v7:
time: 78.6 us; the launch traced here: 78.4 us
  Pallas kernels  77.1 us (98%)
    pallas_call x1, Pallas kernels, shards(): pl.pallas_call(functools.partial(kernel, dims), out_shape=jax.ShapeDtypeS...  77.1 us

profile of v7, /device:TPU:1, one launch (start us, length us, event | category | flops | bytes accessed | tf_op | source)
XLA Modules:
  0.0 78.4 jit_solution(14213587455989206450)
XLA Ops:
  0.7 77.1 %layer.1 = bf16[128,128]{1,0:T(8,128)(2,1)S(1)} custom-call(bf16[128,128]{1,0:T(8,128)(2,1)} %refs_0_.1, bf16[128,128]{1,0:T(8,128)(2,1)} %refs_1_.1, bf16[128,128]{1,0:T(8,128)(2,1)} %refs_2_.1, f32[1,128]{1,0:T(1,128)} %refs_3_.1, f32[1,128]{1,0:T(1,128)} %refs_4_.1, f32[1,128]{1,0:T(1,128)} %refs_5_.1, s32[1,128]{1,0:T(1,128)} %bitcast.18, ...), custom_call_target="tpu_custom_call" | custom-call | tf_op jit(solution)/shard_map/layer/pallas_call | solution.py:630
  77.8 0.6 copy.24

commit v8 on v6

--- a/solution.py
+++ b/solution.py
@@ -57,7 +57,7 @@
         sent, arrived, told, heard, gathered, acc_g, acc_s,
         part2, pair2, send2, recv2,
         rsend, returned, undo, widen,
-        load_sem, pa_s, pa_r, pb_s,
+        met, load_sem, pa_s, pa_r, pb_s,
         near1_r, far1_r, gone1_s, mean_s, sq1_s, sq2_s,
         dis_s, note_s, ret_s, wire_r, own_r, gone_s,
         near2_r, far2_r, gone2_s,
@@ -94,10 +94,16 @@
     def beside(dz, dx):
         return lax.rem(z + dz, nz) * nx + lax.rem(x + dx, nx)
 
-    for dz, dx in hops:
+    lines = [d for d in hops if not (d[0] and d[1])]
+    for dz, dx in lines:
         pl.semaphore_signal(
             barrier, inc=1, device_id=at_sp(beside(dz, dx)), device_id_type=MESH
         )
+    for k in range(1, REACH + 1):
+        for to in (s + k, s - k + n_sp):
+            pl.semaphore_signal(
+                barrier, inc=1, device_id=at_sp(lax.rem(to, n_sp)), device_id_type=MESH
+            )
     for k in sorted(range(1, n_tp), key=lambda k: -min(k, n_tp - k)):
         pl.semaphore_signal(
             barrier, inc=1, device_id=at_tp(lax.rem(t + k, n_tp)), device_id_type=MESH
@@ -178,7 +184,7 @@
     pay[width : width + 8, :] = jnp.broadcast_to(label_first, (8, width)).astype(BF16)
     pay[width + 8 : marks_at, :] = jnp.broadcast_to(label_last, (8, width)).astype(BF16)
     pay[marks_at:, :] = state_map
-    pl.semaphore_wait(barrier, n_sp + n_tp - 2)
+    pl.semaphore_wait(barrier, len(lines) + 2 * REACH + n_tp - 1)
     tops = [pay.shape[0]] * (REACH - 1) + [marks_at]
     first = [
         remote(
@@ -187,8 +193,11 @@
         )
         for k, top in enumerate(tops)
     ]
-    for k in reversed(range(REACH)):
+    for k in (1, 2, 0):
         first[k].start()
+
+    for dz in range(1, nz):
+        pl.semaphore_signal(met, inc=1, device_id=at_sp(beside(dz, 0)), device_id_type=MESH)
 
     for name in names:
         if name not in early:
@@ -412,6 +421,8 @@
     gained = (centred * vm["gain1"][...]).astype(BF16)
     payload = jnp.dot(dispatch, gained, preferred_element_type=F32)
     sent[...] = payload.astype(BF16).reshape(n_sp, stride, rows)
+    if nz > 1:
+        pl.semaphore_wait(met, nz - 1)
     scatter(sent, arrived, dis_s)
     tell(stat1, sq1_s, to_row(jnp.sum(centred * centred, -1, keepdims=True)))
     came = collected(arrived, dis_s)
@@ -647,7 +658,7 @@
             vmem(7, slots, width),
             vmem(n_sp, stride, width), vmem(n_sp, stride, width),
             vmem(rows, n_sp * stride), vmem(n_sp * stride, slots),
-            dma((len(operands),)), dma((REACH,)), dma((REACH,)), dma((2,)),
+            pltpu.SemaphoreType.REGULAR, dma((len(operands),)), dma((REACH,)), dma((REACH,)), dma((2,)),
             dma((2 * CHUNKS,)), dma((2 * CHUNKS,)), dma((2,)), dma((2,)), dma((2,)), dma((2,)),
             dma((2,)), dma((2,)), dma((2,)), dma((3 * CHUNKS,)), dma((4 * CHUNKS,)),
             dma((2,)), dma((2 * CHUNKS,)), dma((2 * CHUNKS,)), dma((2,)),

time: 78.4 us -> 78 us (level)
  no operation moved by 1% of the time
where the time goes in v8:
time: 78 us; the launch traced here: 77.9 us
  Pallas kernels  76.6 us (98%)
    pallas_call x1, Pallas kernels, shards(): pl.pallas_call(functools.partial(kernel, dims), out_shape=jax.ShapeDtypeS...  76.6 us

profile of v8, /device:TPU:1, one launch (start us, length us, event | category | flops | bytes accessed | tf_op | source)
XLA Modules:
  0.0 77.9 jit_solution(12669373798350302805)
XLA Ops:
  0.7 76.6 %layer.1 = bf16[128,128]{1,0:T(8,128)(2,1)S(1)} custom-call(bf16[128,128]{1,0:T(8,128)(2,1)} %refs_0_.1, bf16[128,128]{1,0:T(8,128)(2,1)} %refs_1_.1, bf16[128,128]{1,0:T(8,128)(2,1)} %refs_2_.1, f32[1,128]{1,0:T(1,128)} %refs_3_.1, f32[1,128]{1,0:T(1,128)} %refs_4_.1, f32[1,128]{1,0:T(1,128)} %refs_5_.1, s32[1,128]{1,0:T(1,128)} %bitcast.18, ...), custom_call_target="tpu_custom_call" | custom-call | tf_op jit(solution)/shard_map/layer/pallas_call | solution.py:641
  77.3 0.6 copy.24
